TPU v7x, 32 devices: a whole 2x2x4 slice. The times are simulated.
32 devices in a mesh: sp: 8 (over z, x), tp: 4 (over y, core).
Axes of the slice: x: 2, y: 2, z: 4, core: 2. Of those that a mesh axis runs over, the one named last changes fastest.
Arguments:
- queries: bfloat16 [1024, 32, 128], P('sp', 'tp'), may hold values from -6 to 6
- keys: bfloat16 [1024, 8, 128], P('sp', 'tp'), may hold values from -6 to 6
- values: bfloat16 [1024, 8, 128], P('sp', 'tp'), may hold values from -6 to 6
- q_gain: float32 [128], replicated, may hold values from 0.2 to 8
- k_gain: float32 [128], replicated, may hold values from 0.2 to 8
- w_out: bfloat16 [4096, 2048], P('tp'), may hold values from -0.09375 to 0.09375
- residual: bfloat16 [1024, 2048], P(('sp', 'tp')), may hold values from -6 to 6
- gain_mix: float32 [2048], replicated, may hold values from 0.1 to 1.9
- gain_pre: float32 [2048], replicated, may hold values from 0.1 to 1.9
- routes: int32 [1024, 4], P(('sp', 'tp')), may hold values from 0 to 7, all different within a row; in each aligned block of 32 rows (0 to 31, 32 to 63, ...) at most 32 rows name the same one
- route_weights: float32 [1024, 4], P(('sp', 'tp')), may hold values from 0.1 to 1
- w_gate: bfloat16 [8, 2048, 2048], P('sp', None, 'tp'), may hold values from -0.5 to 0.5
- w_up: bfloat16 [8, 2048, 2048], P('sp', None, 'tp'), may hold values from -0.5 to 0.5
- w_down: bfloat16 [8, 2048, 2048], P('sp', 'tp'), may hold values from -0.125 to 0.125
- gain_moe: float32 [2048], replicated, may hold values from 0.1 to 1.9
Outputs:
- layer_out: bfloat16 [1024, 2048], P(('sp', 'tp'))
Inputs may be any that keep to these rules, and one draw needn't show every extreme that they name: `routes`: each row names 4 different experts. In each aligned block of 32 rows (the rows of one device) no expert is named by more than 32 rows, a bound that some block reaches.
All inputs are finite; a program needn't handle non-finite values.
Results may differ from a plain program's by a relative error of at most 0.017.
The roundings to bfloat16 on the way count: a program that leaves them out, or rounds other values in their place, can miss the bound.
Values may be sent and summed in bfloat16 or wider, within the bound.
A program may use at most 128 MiB of HBM per device.

v0:
```python
import functools
import math

import jax
import jax.numpy as jnp
from jax import lax
from jax.experimental import pallas as pl
from jax.experimental.pallas import tpu as pltpu
from jax.sharding import PartitionSpec as P

TOP = 4
GRID_W = 64


norm_eps = 1e-06
rope_theta = 10000.0
clamp_limit = 7.0
swish_alpha = 1.702


def rope_tables(positions, head_size):
    row_index = (positions // GRID_W).astype(jnp.float32)
    col_index = (positions % GRID_W).astype(jnp.float32)
    freq_count = head_size // 4
    inverse = rope_theta ** (-jnp.arange(freq_count, dtype=jnp.float32) / freq_count)
    angles = jnp.stack([row_index[:, None] * inverse, col_index[:, None] * inverse], axis=1)
    return (jnp.cos(angles), jnp.sin(angles))


def turn(array_in, cosine_table, sine_table):
    token_count, head_count, head_size = array_in.shape
    split_field = array_in.reshape(token_count, head_count, 2, 2, head_size // 4)
    first_half = split_field[:, :, :, 0, :]
    second_half = split_field[:, :, :, 1, :]
    cos_wide = cosine_table[:, None]
    sin_wide = sine_table[:, None]
    turned = jnp.stack(
        [
            first_half * cos_wide - second_half * sin_wide,
            second_half * cos_wide + first_half * sin_wide,
        ],
        axis=3,
    )
    return turned.reshape(token_count, head_count, head_size)


def scale_rows(array_in, gain_vec):
    return (
        array_in
        * lax.rsqrt(jnp.mean(array_in * array_in, axis=-1, keepdims=True) + norm_eps)
        * gain_vec
    )


def slot_table(route_rows, experts, capacity):
    flat_routes = route_rows.reshape(-1)
    expert_hits = (flat_routes[:, None] == jnp.arange(experts, dtype=jnp.int32)[None, :]).astype(
        jnp.int32
    )
    slot_index = jnp.sum((jnp.cumsum(expert_hits, axis=0) - expert_hits) * expert_hits, axis=1)
    target = flat_routes * capacity + slot_index
    slot_onehot = target[:, None] == jnp.arange(experts * capacity, dtype=jnp.int32)[None, :]
    return slot_onehot.astype(jnp.bfloat16).reshape(
        route_rows.shape[0], route_rows.shape[1], experts * capacity
    )


def expert_apply(arrived_rows, w_gate, w_up, w_down):
    gate_pre = jnp.minimum(
        jnp.einsum("serd,edf->serf", arrived_rows, w_gate, preferred_element_type=jnp.float32),
        clamp_limit,
    )
    up_pre = jnp.clip(
        jnp.einsum("serd,edf->serf", arrived_rows, w_up, preferred_element_type=jnp.float32),
        -clamp_limit,
        clamp_limit,
    )
    active = (gate_pre * jax.nn.sigmoid(swish_alpha * gate_pre) * (up_pre + 1.0)).astype(
        jnp.bfloat16
    )
    partial_value = jnp.einsum("serf,efd->serd", active, w_down, preferred_element_type=jnp.float32)
    return lax.optimization_barrier(partial_value.astype(jnp.bfloat16)).astype(jnp.float32)


def send_back(finished):
    return lax.all_to_all(finished, "sp", split_axis=0, concat_axis=0, tiled=True)


MESH = pl.DeviceIdType.MESH
RING = 4
PAIR = 2
LANES = 128


def gather_kernel(n, own_ref, out_ref, send_sem, recv_sem, pass_sem, take_sem, own_sem):
    me = lax.axis_index("sp")
    tp = lax.axis_index("tp")
    pair = me + 1 - 2 * lax.rem(me, 2)
    barrier = pltpu.get_barrier_semaphore()

    def greet(i, carry):
        pl.semaphore_signal(
            barrier, inc=1, device_id=(lax.rem(me + 2 * i, n), tp), device_id_type=MESH
        )
        return carry

    lax.fori_loop(1, n // 2, greet, 0)
    pl.semaphore_signal(barrier, inc=1, device_id=(pair, tp), device_id_type=MESH)
    keep = pltpu.make_async_copy(own_ref, out_ref.at[me], own_sem)
    keep.start()
    pl.semaphore_wait(barrier, n // 2)

    def along(i):
        return pltpu.make_async_remote_copy(
            src_ref=own_ref,
            dst_ref=out_ref.at[me],
            send_sem=send_sem.at[i],
            recv_sem=recv_sem.at[i],
            device_id=(lax.rem(me + 2 * i, n), tp),
            device_id_type=MESH,
        )

    def across(i, src):
        return pltpu.make_async_remote_copy(
            src_ref=src,
            dst_ref=out_ref.at[lax.rem(me + n - 2 * i, n)],
            send_sem=pass_sem.at[i],
            recv_sem=take_sem.at[i],
            device_id=(pair, tp),
            device_id_type=MESH,
        )

    def relay(i):
        return across(i, out_ref.at[lax.rem(me + n - 2 * i, n)])

    def start(i, carry):
        along(i).start()
        return carry

    def forward(i, carry):
        along(i).wait_recv()
        relay(i).start()
        return carry

    def finish(i, carry):
        along(i).wait_send()
        relay(i).wait()
        return carry

    lax.fori_loop(1, n // 2, start, 0)
    across(0, own_ref).start()
    keep.wait()
    lax.fori_loop(1, n // 2, forward, 0)
    across(0, own_ref).wait()
    lax.fori_loop(1, n // 2, finish, 0)


def gather_sp(block):
    n = lax.axis_size("sp")
    return pl.pallas_call(
        functools.partial(gather_kernel, n),
        out_shape=jax.ShapeDtypeStruct((n,) + block.shape, block.dtype),
        in_specs=[pl.BlockSpec(memory_space=pltpu.VMEM)],
        out_specs=pl.BlockSpec(memory_space=pltpu.VMEM),
        scratch_shapes=[
            pltpu.SemaphoreType.DMA((n // 2,)),
            pltpu.SemaphoreType.DMA((n // 2,)),
            pltpu.SemaphoreType.DMA((n // 2,)),
            pltpu.SemaphoreType.DMA((n // 2,)),
            pltpu.SemaphoreType.DMA,
        ],
        compiler_params=pltpu.CompilerParams(collective_id=0, has_side_effects=True),
        cost_estimate=pl.CostEstimate(flops=0, bytes_accessed=1 << 24, transcendentals=0),
        name="gather_kv",
    )(block)


def wide(value):
    return value.astype(jnp.float32)


def experts_kernel(
    part, residual, gain_mix, gain_pre, gain_moe, tail, wg_hbm, wu_hbm, wd_hbm, out,
    wg, wu, wd, got, middle, rows, active, partial, core_in, summed, far_in, near_in,
    x_in, y_in, w_sem, part_s, part_r, y_s, y_r, x_s, x_r, z_s, z_r, q_s, q_r, c_s, c_r,
    rc_s, rc_r, e_s, e_r, f_s, f_r, l_s, l_r, rx_s, rx_r, ry_s, ry_r,
):
    sp = lax.axis_index("sp")
    tp = lax.axis_index("tp")
    z, x = sp // PAIR, lax.rem(sp, PAIR)
    y, c = tp // PAIR, lax.rem(tp, PAIR)
    ox, oy, oc = 1 - x, 1 - y, 1 - c
    zp, zm, zq = lax.rem(z + 1, RING), lax.rem(z + 3, RING), lax.rem(z + 2, RING)
    width = residual.shape[1]
    to_c = (sp, y * PAIR + oc)
    to_y = (sp, oy * PAIR + c)
    to_yc = (sp, oy * PAIR + oc)
    to_x = (z * PAIR + ox, tp)
    to_zp = (zp * PAIR + x, tp)
    to_zm = (zm * PAIR + x, tp)
    peers = (to_c, to_y, to_yc, to_x, to_zp, to_zm)

    loads = [
        pltpu.make_async_copy(a, b, w_sem.at[i])
        for i, (a, b) in enumerate(((wg_hbm, wg), (wu_hbm, wu), (wd_hbm, wd)))
    ]
    for load in loads:
        load.start()
    barrier = pltpu.get_barrier_semaphore()
    for peer in peers:
        pl.semaphore_signal(barrier, inc=1, device_id=peer, device_id_type=MESH)
    pl.semaphore_wait(barrier, len(peers))

    started = []

    def send(src, dst, s, r, to):
        copy = pltpu.make_async_remote_copy(
            src_ref=src, dst_ref=dst, send_sem=s, recv_sem=r, device_id=to, device_id_type=MESH
        )
        copy.start()
        started.append(copy)
        return copy

    with jax.named_scope("proj"):
        copies = [
            send(part.at[to[1]], core_in.at[0, i], part_s.at[i], part_r.at[i], to)
            for i, to in ((2, to_yc), (1, to_y), (0, to_c))
        ]
        for copy in copies:
            copy.wait_recv()
        projected = wide(part[tp])
        for i in range(3):
            projected = projected + wide(core_in[0, i])
        mid = wide(residual[...]) + scale_rows(projected, gain_mix[...])
        middle[...] = mid
        mine = x * PAIR + y
        got[z, c, mine, :, 0:width] = scale_rows(mid, gain_pre[...]).astype(jnp.bfloat16)
        got[z, c, mine, :, width:] = tail[...]

    blk = (mine, x * PAIR + oy, ox * PAIR + y, ox * PAIR + oy)
    groups = (z, zm, zp, zq)

    def block(g, k):
        return got.at[groups[g], c, blk[k]]

    def relay(g, k):
        return send(block(g, k), block(g, k), c_s.at[g, k], c_r.at[g, k], to_c)

    relays = [[None] * 4 for _ in range(4)]
    plus, minus = [None] * 4, [None] * 4
    far = [None] * 4

    def spread(k):
        plus[k] = send(block(0, k), block(0, k), z_s.at[0, k], z_r.at[0, k], to_zp)
        minus[k] = send(block(0, k), block(0, k), z_s.at[1, k], z_r.at[1, k], to_zm)
        relays[0][k] = relay(0, k)

    with jax.named_scope("spread"):
        ycopy = send(block(0, 0), block(0, 0), y_s.at[0], y_r.at[0], to_y)
        xcopy0 = send(block(0, 0), block(0, 0), x_s.at[0], x_r.at[0], to_x)
        spread(0)
        ycopy.wait_recv()
        xcopy1 = send(block(0, 1), block(0, 1), x_s.at[1], x_r.at[1], to_x)
        spread(1)
        xcopy0.wait_recv()
        spread(2)
        xcopy1.wait_recv()
        spread(3)

    per = got.shape[2] * got.shape[3]

    def serve(g):
        group = groups[g]
        arrived = got[group].reshape(2 * per, got.shape[4])
        rows[...] = arrived
        spread_w = wide(rows[:, width:])
        lane = lax.broadcasted_iota(jnp.int32, spread_w.shape, 1)
        chosen = lax.rem(lane, spread_w.shape[1] // 2) == sp
        coef = jnp.sum(jnp.where(chosen, spread_w, 0.0), axis=1, keepdims=True)
        step = min(wg.shape[1], 256)

        @pl.loop(0, wg.shape[1] // step)
        def _(i):
            cols = pl.ds(pl.multiple_of(i * step, step), step)
            gate = jnp.dot(rows[:, 0:width], wg[:, cols], preferred_element_type=jnp.float32)
            up = jnp.dot(rows[:, 0:width], wu[:, cols], preferred_element_type=jnp.float32)
            gate = jnp.minimum(gate, clamp_limit)
            up = jnp.clip(up, -clamp_limit, clamp_limit)
            active[:, cols] = (gate * jax.nn.sigmoid(swish_alpha * gate) * (up + 1.0)).astype(
                jnp.bfloat16
            )

        @pl.loop(0, width // 512)
        def _(i):
            cols = pl.ds(pl.multiple_of(i * 512, 512), 512)
            down = jnp.dot(active[...], wd[:, cols], preferred_element_type=jnp.float32)
            partial[g, :, :, :, cols] = (
                (down * coef).astype(jnp.bfloat16).reshape(partial.shape[1:4] + (512,))
            )

        return send(partial.at[g, oc], core_in.at[g], rc_s.at[g], rc_r.at[g], to_c)

    def fold(g, copy):
        copy.wait_recv()
        for k in range(4):
            summed[g, k] = (wide(partial[g, c, k]) + wide(core_in[g, k])).astype(jnp.bfloat16)

    def await_core(g):
        for k in range(4):
            relays[g][k].wait_recv()

    half_a, half_b = pl.ds(x * PAIR, PAIR), pl.ds(ox * PAIR, PAIR)

    for load in loads:
        load.wait()
    with jax.named_scope("own"):
        await_core(0)
        back0 = serve(0)
    with jax.named_scope("near"):
        for k in range(4):
            plus[k].wait_recv()
            if k < 2:
                far[k] = send(block(1, k), block(1, k), q_s.at[k], q_r.at[k], to_zp)
            relays[1][k] = relay(1, k)
            minus[k].wait_recv()
            if k >= 2:
                far[k] = send(block(2, k), block(2, k), q_s.at[k], q_r.at[k], to_zm)
            relays[2][k] = relay(2, k)
        await_core(1)
        back1 = serve(1)
        fold(0, back0)
        for k in range(4):
            far[k].wait_recv()
            relays[3][k] = relay(3, k)
        await_core(2)
        back2 = serve(2)
        fold(1, back1)
        early_m = send(
            summed.at[1, half_a], near_in.at[1, half_a], e_s.at[1], e_r.at[1], to_zm
        )
    with jax.named_scope("far"):
        await_core(3)
        back3 = serve(3)
        fold(2, back2)
        early_p = send(
            summed.at[2, half_b], near_in.at[0, half_b], e_s.at[0], e_r.at[0], to_zp
        )
        fold(3, back3)
        far_p = send(summed.at[3, half_a], far_in.at[0], f_s.at[0], f_r.at[0], to_zp)
        far_m = send(summed.at[3, half_b], far_in.at[1], f_s.at[1], f_r.at[1], to_zm)
    with jax.named_scope("back"):
        far_p.wait_recv()
        for k in range(2):
            place = x * PAIR + k
            summed[2, place] = (wide(summed[2, place]) + wide(far_in[0, k])).astype(jnp.bfloat16)
        late_p = send(
            summed.at[2, half_a], near_in.at[0, half_a], l_s.at[0], l_r.at[0], to_zp
        )
        far_m.wait_recv()
        for k in range(2):
            place = ox * PAIR + k
            summed[1, place] = (wide(summed[1, place]) + wide(far_in[1, k])).astype(jnp.bfloat16)
        late_m = send(
            summed.at[1, half_b], near_in.at[1, half_b], l_s.at[1], l_r.at[1], to_zm
        )

        def total(place):
            return wide(summed[0, place]) + wide(near_in[0, place]) + wide(near_in[1, place])

        early_p.wait_recv()
        early_m.wait_recv()
        late_m.wait_recv()
        late_p.wait_recv()
        for k in range(2):
            place = ox * PAIR + k
            summed[0, place] = total(place).astype(jnp.bfloat16)
        xback = send(summed.at[0, half_b], x_in, rx_s.at[0], rx_r.at[0], to_x)
        xback.wait_recv()
        summed[0, blk[1]] = (total(blk[1]) + wide(x_in[oy])).astype(jnp.bfloat16)
        yback = send(summed.at[0, blk[1]], y_in, ry_s.at[0], ry_r.at[0], to_y)
        keep = total(mine) + wide(x_in[y])
        yback.wait_recv()
        mixture = keep + wide(y_in[...])
        out[...] = (middle[...] + scale_rows(mixture, gain_moe[...])).astype(out.dtype)
        for copy in started:
            copy.wait_send()


def experts_layer(part, residual, gain_mix, gain_pre, gain_moe, tail, w_gate, w_up, w_down):
    tok, width = residual.shape
    ff = w_gate.shape[1]
    full = width + tail.shape[1]
    blocks = PAIR * PAIR
    bf, f32 = jnp.bfloat16, jnp.float32
    dma = pltpu.SemaphoreType.DMA
    here = pl.BlockSpec(memory_space=pltpu.VMEM)
    there = pl.BlockSpec(memory_space=pl.ANY)
    sems = []
    for dims in (
        (3,), (1,), (2,), (2, 4), (4,), (4, 4), (4,), (2,), (2,), (2,), (1,), (1,)
    ):
        sems += [dma(dims), dma(dims)]
    return pl.pallas_call(
        experts_kernel,
        out_shape=jax.ShapeDtypeStruct((tok, width), bf),
        in_specs=[here] * 6 + [there] * 3,
        out_specs=here,
        scratch_shapes=[
            pltpu.VMEM((width, ff), bf),
            pltpu.VMEM((width, ff), bf),
            pltpu.VMEM((ff, width), bf),
            pltpu.VMEM((RING, PAIR, blocks, tok, full), bf),
            pltpu.VMEM((tok, width), f32),
            pltpu.VMEM((PAIR * blocks * tok, full), bf),
            pltpu.VMEM((PAIR * blocks * tok, ff), bf),
            pltpu.VMEM((RING, PAIR, blocks, tok, width), bf),
            pltpu.VMEM((RING, blocks, tok, width), bf),
            pltpu.VMEM((RING, blocks, tok, width), bf),
            pltpu.VMEM((2, PAIR, tok, width), bf),
            pltpu.VMEM((2, blocks, tok, width), bf),
            pltpu.VMEM((PAIR, tok, width), bf),
            pltpu.VMEM((tok, width), bf),
            dma((3,)),
        ]
        + sems,
        compiler_params=pltpu.CompilerParams(
            collective_id=1, has_side_effects=True, vmem_limit_bytes=56 << 20
        ),
        name="experts_layer",
    )(part, residual, gain_mix, gain_pre, gain_moe, tail, w_gate, w_up, w_down)


def weight_tail(routes, route_weights, experts):
    hits = routes[:, :, None] == jnp.arange(experts, dtype=jnp.int32)[None, None, :]
    coef = jnp.sum(jnp.where(hits, route_weights[:, :, None], 0.0), axis=1)
    high = lax.reduce_precision(coef, 8, 7)
    low = coef - high
    gap = jnp.zeros((coef.shape[0], LANES // 2 - experts), jnp.float32)
    return jnp.concatenate([high, gap, low, gap], axis=1).astype(jnp.bfloat16)


def on_device(
    queries,
    keys,
    values,
    q_gain,
    k_gain,
    w_out,
    residual,
    gain_mix,
    gain_pre,
    routes,
    route_weights,
    w_gate,
    w_up,
    w_down,
    gain_moe,
):
    tok_rows, head_local, head_size = queries.shape
    kv_local = keys.shape[1]
    group_size = head_local // kv_local
    positions = lax.axis_index("sp") * tok_rows + jnp.arange(tok_rows, dtype=jnp.int32)
    cosine_table, sine_table = rope_tables(positions, head_size)
    q_turned = (
        turn(scale_rows(queries.astype(jnp.float32), q_gain), cosine_table, sine_table)
        * head_size ** (-0.5)
    ).astype(jnp.bfloat16)
    k_turned = turn(scale_rows(keys.astype(jnp.float32), k_gain), cosine_table, sine_table).astype(
        jnp.bfloat16
    )
    q_grouped = q_turned.reshape(tok_rows, kv_local, group_size, head_size)
    initial = (
        jnp.full((kv_local, group_size, tok_rows), -jnp.inf, jnp.float32),
        jnp.zeros((kv_local, group_size, tok_rows), jnp.float32),
        jnp.zeros((kv_local, group_size, tok_rows, head_size), jnp.float32),
    )
    carry_state = initial
    kv_cols = kv_local * head_size
    both = gather_sp(
        jnp.concatenate(
            [k_turned.reshape(tok_rows, kv_cols), values.reshape(tok_rows, kv_cols)], axis=1
        )
    ).reshape(-1, 2 * kv_cols)
    key_piece = both[:, :kv_cols].reshape(-1, kv_local, head_size)
    value_piece = both[:, kv_cols:].reshape(-1, kv_local, head_size)
    piece_rows = key_piece.shape[0]
    block_rows = math.gcd(piece_rows, 1024)
    key_blocks = key_piece.reshape(piece_rows // block_rows, block_rows, kv_local, head_size)
    value_blocks = value_piece.reshape(piece_rows // block_rows, block_rows, kv_local, head_size)

    def absorb_block(state_now, key_value):
        running_max, running_sum, weighted = state_now
        key_block, value_block = key_value
        scores = jnp.einsum(
            "qkgd,skd->kgqs", q_grouped, key_block, preferred_element_type=jnp.float32
        )
        new_max = jnp.maximum(running_max, jnp.max(scores, axis=-1))
        rescale = jnp.exp(running_max - new_max)
        unnorm = jnp.exp(scores - new_max[..., None])
        running_sum = running_sum * rescale + jnp.sum(unnorm, axis=-1)
        weighted = weighted * rescale[..., None] + jnp.einsum(
            "kgqs,skd->kgqd",
            unnorm.astype(jnp.bfloat16),
            value_block,
            preferred_element_type=jnp.float32,
        )
        return ((new_max, running_sum, weighted), None)

    carry_state, ignored = lax.scan(absorb_block, carry_state, (key_blocks, value_blocks))
    running_max, running_sum, weighted = carry_state
    mixed_heads = (weighted / running_sum[..., None]).transpose(2, 0, 1, 3)
    mixed_heads = mixed_heads.reshape(tok_rows, head_local * head_size).astype(jnp.bfloat16)
    tok_part = residual.shape[0]
    width = residual.shape[1]
    part = jnp.dot(mixed_heads, w_out, preferred_element_type=jnp.float32).astype(jnp.bfloat16)
    local_experts = w_gate.shape[0]
    experts_all = local_experts * lax.axis_size("sp")
    capacity = max(2, (2 * tok_part * TOP + experts_all - 1) // experts_all)
    grid_fits = lax.axis_size("sp") == RING * PAIR and lax.axis_size("tp") == PAIR * PAIR
    if grid_fits and local_experts == 1 and capacity >= tok_part:
        return experts_layer(
            part.reshape(PAIR * PAIR, tok_part, width),
            residual,
            gain_mix[None],
            gain_pre[None],
            gain_moe[None],
            weight_tail(routes, route_weights, experts_all),
            w_gate[0],
            w_up[0],
            w_down[0],
        )
    projected = lax.psum_scatter(
        part,
        "tp",
        scatter_dimension=0,
        tiled=True,
    ).astype(jnp.float32)
    middle = residual.astype(jnp.float32) + scale_rows(projected, gain_mix)
    normed = scale_rows(middle, gain_pre).astype(jnp.bfloat16)
    tables = slot_table(routes, experts_all, capacity)
    chosen = jnp.sum(tables, axis=1)
    outbound = jnp.einsum("tp,td->pd", chosen, normed, preferred_element_type=jnp.float32)
    outbound = outbound.astype(jnp.bfloat16).reshape(experts_all, capacity, width)
    arrived_rows = lax.all_gather(
        lax.all_to_all(outbound, "sp", split_axis=0, concat_axis=0, tiled=True),
        "tp",
        axis=0,
        tiled=True,
    )
    leading = arrived_rows.shape[0] // local_experts
    partial_value = expert_apply(
        arrived_rows.reshape(leading, local_experts, arrived_rows.shape[1], width),
        w_gate,
        w_up,
        w_down,
    )
    summed = lax.psum_scatter(
        partial_value.reshape(arrived_rows.shape).astype(jnp.bfloat16),
        "tp",
        scatter_dimension=0,
        tiled=True,
    )
    returned = send_back(summed)
    gathered = jnp.einsum(
        "tkp,pd->tkd",
        tables,
        returned.reshape(experts_all * capacity, width),
        preferred_element_type=jnp.float32,
    )
    mixture = jnp.sum(gathered * route_weights[:, :, None], axis=1)
    return (middle + scale_rows(mixture, gain_moe)).astype(jnp.bfloat16)


def solution(mesh):
    placed = (
        P("sp", "tp", None),
        P("sp", "tp", None),
        P("sp", "tp", None),
        P(),
        P(),
        P("tp", None),
        P(("sp", "tp"), None),
        P(),
        P(),
        P(("sp", "tp"), None),
        P(("sp", "tp"), None),
        P("sp", None, "tp"),
        P("sp", None, "tp"),
        P("sp", "tp", None),
        P(),
    )
    return jax.shard_map(
        on_device, mesh=mesh, in_specs=placed, out_specs=P(("sp", "tp"), None), check_vma=False
    )
```

profile of v0, /device:TPU:0, one launch (start us, length us, event | category | flops | bytes accessed | tf_op | source)
XLA Modules:
  0.0 137.3 jit_solution(2355510117371056078)
XLA Ops:
  0.0 0.9 copy.62
  0.9 1.0 copy.42
  1.9 0.7 fusion.22
  2.7 0.1 broadcast_multiply_fusion.1
  2.8 0.1 fusion.24
  3.0 0.1 copy.43
  3.1 0.7 pad_maximum_fusion.own_ref
  3.7 24.5 %gather_kv.1 = bf16[8,128,512]{2,1,0:T(8,128)(2,1)} custom-call(bf16[128,512]{1,0:T(8,128)(2,1)} %pad_maximum_fusion.own_ref), custom_call_target="tpu_custom_call" | custom-call | bytes 16777216 | tf_op jit(solution)/shard_map/gather_kv/pallas_call | solution.py:160
  28.2 1.3 fusion.27
  29.5 0.2 copy.48
  29.7 0.2 copy.59
  29.9 0.2 copy.45
  30.3 0.1 fusion.19
  30.4 0.1 multiply_subtract_fusion
  30.5 0.8 bitcast_reduce_fusion
  31.3 0.6 fusion.1
  31.9 0.9 fusion.15
  32.9 0.6 copy-done
  33.5 1.5 %convolution_convert_fusion = bf16[128,2048]{1,0:T(8,128)(2,1)} fusion(bf16[128,1024]{0,1:T(8,128)(2,1)S(1)} %bitcast.74, bf16[1024,2048]{1,0:T(8,128)(2,1)S(1)} %copy-done), kind=kOutput, calls=%fused_computation.5 | convolution fusion | flops 537133056 | bytes 4980736 | tf_op jit(solution)/shard_map/dot_general | solution.py:515
  35.1 0.1 copy.50
  35.1 0.1 copy.51
  35.2 0.7 pad_maximum_fusion.3.tail
  35.9 99.8 %experts_layer.1 = bf16[32,2048]{1,0:T(8,128)(2,1)} custom-call(bf16[4,32,2048]{2,1,0:T(8,128)(2,1)} %bitcast.68, bf16[32,2048]{1,0:T(8,128)(2,1)} %residual.1, f32[1,2048]{1,0:T(1,128)} %bitcast.78, f32[1,2048]{1,0:T(1,128)} %bitcast.79, f32[1,2048]{1,0:T(1,128)} %bitcast.80, bf16[32,128]{1,0:T(8,128)(2,1)} %pad_maximum_fusion.3.tail, ...), custom_call_target="tpu_custom_call" | custom-call | tf_op jit(solution)/shard_map/experts_layer/pallas_call | solution.py:403
  135.7 1.6 %copy.64 = bf16[32,2048]{1,0:T(8,128)(2,1)} copy(bf16[32,2048]{1,0:T(8,128)(2,1)} %experts_layer.1) | data formatting | bytes 262144
  (24 shorter events, 0.3 us)
Async XLA Ops:
  0.0 29.9 %copy-start.1 = (bf16[128,8,128]{2,1,0:T(8,128)(2,1)S(1)}, bf16[128,8,128]{2,1,0:T(8,128)(2,1)}, u32[]{:S(2)}) copy-start(bf16[128,8,128]{2,1,0:T(8,128)(2,1)} %param.15) | copy-start | bytes 786436
  0.0 30.2 %copy-start.4 = (f32[128]{0:T(128)S(1)}, f32[128]{0:T(128)}, u32[]{:S(2)}) copy-start(f32[128]{0:T(128)} %param.18) | copy-start | bytes 1540
  31.3 2.2 %copy-start = (bf16[1024,2048]{1,0:T(8,128)(2,1)S(1)}, bf16[1024,2048]{1,0:T(8,128)(2,1)}, u32[]{:S(2)}) copy-start(bf16[1024,2048]{1,0:T(8,128)(2,1)} %param.20) | copy-start | bytes 12582916
  31.9 3.1 %copy-start.2 = (f32[32,4]{0,1:T(4,128)S(1)}, f32[32,4]{0,1:T(4,128)}, u32[]{:S(2)}) copy-start(f32[32,4]{0,1:T(4,128)} %param.25) | copy-start | bytes 1540
  31.9 3.1 %copy-start.3 = (s32[32,4]{0,1:T(4,128)S(1)}, s32[32,4]{0,1:T(4,128)}, u32[]{:S(2)}) copy-start(s32[32,4]{0,1:T(4,128)} %param.24) | copy-start | bytes 1540
where the time goes:
time: 138 us; the launch traced here: 137 us
  Pallas kernels  124 us (90%)
  local copies, waits for them, and re-layouts  6.26 us (5%)
  other arithmetic  3.31 us (2%)
  matrix products  3.2 us (2%)
    pallas_call x1, Pallas kernels, experts_layer(): pl.pallas_call(experts_kernel, out_shape=jax.ShapeDtypeStruct((tok, width...  99.8 us
    pallas_call x1, Pallas kernels, gather_sp(): pl.pallas_call(functools.partial(gather_kernel, n), out_shape=jax.ShapeDt...  24.5 us
    unnamed x15, local copies, waits for them, and re-layouts  4.52 us

commit v1 on v0

--- a/solution.py
+++ b/solution.py
@@ -1,5 +1,6 @@
 import functools
 import math
+from types import SimpleNamespace
 
 import jax
 import jax.numpy as jnp
@@ -179,30 +180,33 @@
     return value.astype(jnp.float32)
 
 
-def experts_kernel(
-    part, residual, gain_mix, gain_pre, gain_moe, tail, wg_hbm, wu_hbm, wd_hbm, out,
-    wg, wu, wd, got, middle, rows, active, partial, core_in, summed, far_in, near_in,
-    x_in, y_in, w_sem, part_s, part_r, y_s, y_r, x_s, x_r, z_s, z_r, q_s, q_r, c_s, c_r,
-    rc_s, rc_r, e_s, e_r, f_s, f_r, l_s, l_r, rx_s, rx_r, ry_s, ry_r,
-):
+def experts_kernel(names, *refs):
+    r = SimpleNamespace(**dict(zip(names, refs)))
     sp = lax.axis_index("sp")
     tp = lax.axis_index("tp")
     z, x = sp // PAIR, lax.rem(sp, PAIR)
     y, c = tp // PAIR, lax.rem(tp, PAIR)
     ox, oy, oc = 1 - x, 1 - y, 1 - c
-    zp, zm, zq = lax.rem(z + 1, RING), lax.rem(z + 3, RING), lax.rem(z + 2, RING)
-    width = residual.shape[1]
+    width = r.residual.shape[1]
+    half = r.residual.shape[0] // 2
+    top, bottom = pl.ds(0, half), pl.ds(half, half)
+    upper = z // 2
+    folded = z + upper * (RING - 1 - 2 * z)
+
+    def plane(o):
+        return o + upper * (RING - 1 - 2 * o)
+
+    groups = (z, plane(folded + 1), plane(2 - 2 * folded), plane(RING - 1))
     to_c = (sp, y * PAIR + oc)
     to_y = (sp, oy * PAIR + c)
-    to_yc = (sp, oy * PAIR + oc)
     to_x = (z * PAIR + ox, tp)
-    to_zp = (zp * PAIR + x, tp)
-    to_zm = (zm * PAIR + x, tp)
-    peers = (to_c, to_y, to_yc, to_x, to_zp, to_zm)
+    to_z = [None] + [(g * PAIR + x, tp) for g in groups[1:]]
+    peers = [to_c, to_y, to_x] + to_z[1:]
+    mine, xb, yb, db = x * PAIR + y, ox * PAIR + y, x * PAIR + oy, ox * PAIR + oy
 
     loads = [
-        pltpu.make_async_copy(a, b, w_sem.at[i])
-        for i, (a, b) in enumerate(((wg_hbm, wg), (wu_hbm, wu), (wd_hbm, wd)))
+        pltpu.make_async_copy(a, b, r.w_sem.at[i])
+        for i, (a, b) in enumerate(((r.wg_hbm, r.wg), (r.wu_hbm, r.wu), (r.wd_hbm, r.wd)))
     ]
     for load in loads:
         load.start()
@@ -213,175 +217,199 @@
 
     started = []
 
-    def send(src, dst, s, r, to):
+    def send(src, dst, s, t, to):
         copy = pltpu.make_async_remote_copy(
-            src_ref=src, dst_ref=dst, send_sem=s, recv_sem=r, device_id=to, device_id_type=MESH
+            src_ref=src, dst_ref=dst, send_sem=s, recv_sem=t, device_id=to, device_id_type=MESH
         )
         copy.start()
         started.append(copy)
         return copy
 
+    def narrow(value):
+        return value.astype(jnp.bfloat16)
+
     with jax.named_scope("proj"):
-        copies = [
-            send(part.at[to[1]], core_in.at[0, i], part_s.at[i], part_r.at[i], to)
-            for i, to in ((2, to_yc), (1, to_y), (0, to_c))
-        ]
-        for copy in copies:
+        first = send(r.part.at[oy, oc], r.pc_in.at[0], r.pc_s.at[0], r.pc_r.at[0], to_c)
+        second = send(r.part.at[y, oc], r.pc_in.at[1], r.pc_s.at[1], r.pc_r.at[1], to_c)
+        first.wait_recv()
+        r.py_out[...] = narrow(wide(r.part[oy, c]) + wide(r.pc_in[0]))
+        third = send(r.py_out, r.py_in, r.py_s.at[0], r.py_r.at[0], to_y)
+        second.wait_recv()
+        projected = wide(r.part[y, c]) + wide(r.pc_in[1])
+        third.wait_recv()
+        projected = projected + wide(r.py_in[...])
+        mid = wide(r.residual[...]) + scale_rows(projected, r.gain_mix[...])
+        r.middle[...] = mid
+        r.got[z, c, mine, :, 0:width] = narrow(scale_rows(mid, r.gain_pre[...]))
+        r.got[z, c, mine, :, width:] = r.tail[...]
+
+    def block(p, k, rows=slice(None)):
+        return r.got.at[groups[p], c, k, rows]
+
+    z_copy, x_copy, y_copy = [None] * 4, [None] * 4, [None] * 4
+    hx_copy, hy_copy = [None] * 4, [None] * 4
+    relays = [[] for _ in range(4)]
+
+    def relay(p, k, slot):
+        relays[p].append(
+            send(block(p, k), block(p, k), r.c_s.at[p, slot], r.c_r.at[p, slot], to_c)
+        )
+
+    def spread(p):
+        if p:
+            pltpu.make_async_remote_copy(
+                src_ref=block(p, mine), dst_ref=block(p, mine), send_sem=r.z_s.at[p],
+                recv_sem=r.z_r.at[groups[p]], device_id=to_z[p], device_id_type=MESH,
+            ).wait_recv()
+        x_copy[p] = send(block(p, mine), block(p, mine), r.x_s.at[p], r.x_r.at[p], to_x)
+        y_copy[p] = send(block(p, mine), block(p, mine), r.y_s.at[p], r.y_r.at[p], to_y)
+        relay(p, mine, 0)
+
+    def cross(p):
+        x_copy[p].wait_recv()
+        hy_copy[p] = send(
+            block(p, xb, top), block(p, xb, top), r.hy_s.at[p], r.hy_r.at[p], to_y
+        )
+        relay(p, xb, 1)
+        y_copy[p].wait_recv()
+        hx_copy[p] = send(
+            block(p, yb, bottom), block(p, yb, bottom), r.hx_s.at[p], r.hx_r.at[p], to_x
+        )
+        relay(p, yb, 2)
+
+    def corner(p):
+        hx_copy[p].wait_recv()
+        hy_copy[p].wait_recv()
+        relay(p, db, 3)
+
+    per = r.got.shape[2] * r.got.shape[3]
+
+    def serve(p):
+        for copy in relays[p]:
             copy.wait_recv()
-        projected = wide(part[tp])
-        for i in range(3):
-            projected = projected + wide(core_in[0, i])
-        mid = wide(residual[...]) + scale_rows(projected, gain_mix[...])
-        middle[...] = mid
-        mine = x * PAIR + y
-        got[z, c, mine, :, 0:width] = scale_rows(mid, gain_pre[...]).astype(jnp.bfloat16)
-        got[z, c, mine, :, width:] = tail[...]
-
-    blk = (mine, x * PAIR + oy, ox * PAIR + y, ox * PAIR + oy)
-    groups = (z, zm, zp, zq)
-
-    def block(g, k):
-        return got.at[groups[g], c, blk[k]]
-
-    def relay(g, k):
-        return send(block(g, k), block(g, k), c_s.at[g, k], c_r.at[g, k], to_c)
-
-    relays = [[None] * 4 for _ in range(4)]
-    plus, minus = [None] * 4, [None] * 4
-    far = [None] * 4
-
-    def spread(k):
-        plus[k] = send(block(0, k), block(0, k), z_s.at[0, k], z_r.at[0, k], to_zp)
-        minus[k] = send(block(0, k), block(0, k), z_s.at[1, k], z_r.at[1, k], to_zm)
-        relays[0][k] = relay(0, k)
-
-    with jax.named_scope("spread"):
-        ycopy = send(block(0, 0), block(0, 0), y_s.at[0], y_r.at[0], to_y)
-        xcopy0 = send(block(0, 0), block(0, 0), x_s.at[0], x_r.at[0], to_x)
-        spread(0)
-        ycopy.wait_recv()
-        xcopy1 = send(block(0, 1), block(0, 1), x_s.at[1], x_r.at[1], to_x)
-        spread(1)
-        xcopy0.wait_recv()
-        spread(2)
-        xcopy1.wait_recv()
-        spread(3)
-
-    per = got.shape[2] * got.shape[3]
-
-    def serve(g):
-        group = groups[g]
-        arrived = got[group].reshape(2 * per, got.shape[4])
-        rows[...] = arrived
-        spread_w = wide(rows[:, width:])
+        g = groups[p]
+        spread_w = wide(r.got[g, :, :, :, width:].reshape(2 * per, LANES))
         lane = lax.broadcasted_iota(jnp.int32, spread_w.shape, 1)
-        chosen = lax.rem(lane, spread_w.shape[1] // 2) == sp
+        chosen = lax.rem(lane, LANES // 2) == sp
         coef = jnp.sum(jnp.where(chosen, spread_w, 0.0), axis=1, keepdims=True)
-        step = min(wg.shape[1], 256)
-
-        @pl.loop(0, wg.shape[1] // step)
+        step = min(r.wg.shape[1], 256)
+
+        @pl.loop(0, r.wg.shape[1] // step)
         def _(i):
             cols = pl.ds(pl.multiple_of(i * step, step), step)
-            gate = jnp.dot(rows[:, 0:width], wg[:, cols], preferred_element_type=jnp.float32)
-            up = jnp.dot(rows[:, 0:width], wu[:, cols], preferred_element_type=jnp.float32)
+            rows = r.got[g, :, :, :, 0:width].reshape(2 * per, width)
+            gate = jnp.dot(rows, r.wg[:, cols], preferred_element_type=jnp.float32)
+            up = jnp.dot(rows, r.wu[:, cols], preferred_element_type=jnp.float32)
             gate = jnp.minimum(gate, clamp_limit)
             up = jnp.clip(up, -clamp_limit, clamp_limit)
-            active[:, cols] = (gate * jax.nn.sigmoid(swish_alpha * gate) * (up + 1.0)).astype(
-                jnp.bfloat16
-            )
+            r.active[:, cols] = narrow(gate * jax.nn.sigmoid(swish_alpha * gate) * (up + 1.0))
 
         @pl.loop(0, width // 512)
         def _(i):
             cols = pl.ds(pl.multiple_of(i * 512, 512), 512)
-            down = jnp.dot(active[...], wd[:, cols], preferred_element_type=jnp.float32)
-            partial[g, :, :, :, cols] = (
-                (down * coef).astype(jnp.bfloat16).reshape(partial.shape[1:4] + (512,))
+            down = jnp.dot(r.active[...], r.wd[:, cols], preferred_element_type=jnp.float32)
+            r.partial[p, :, :, :, cols] = narrow(down * coef).reshape(
+                r.partial.shape[1:4] + (512,)
             )
 
-        return send(partial.at[g, oc], core_in.at[g], rc_s.at[g], rc_r.at[g], to_c)
-
-    def fold(g, copy):
-        copy.wait_recv()
-        for k in range(4):
-            summed[g, k] = (wide(partial[g, c, k]) + wide(core_in[g, k])).astype(jnp.bfloat16)
-
-    def await_core(g):
-        for k in range(4):
-            relays[g][k].wait_recv()
-
-    half_a, half_b = pl.ds(x * PAIR, PAIR), pl.ds(ox * PAIR, PAIR)
-
+        back[p] = send(r.partial.at[p, oc], r.core_in.at[p], r.rc_s.at[p], r.rc_r.at[p], to_c)
+
+    back = [None] * 4
+    dx_copy, dy_copy = [None] * 4, [None] * 4
+    bx_copy, by_copy = [[] for _ in range(4)], [[] for _ in range(4)]
+    home = [None] * 4
+
+    def give_x(p, i, rows):
+        bx_copy[p].append(
+            send(
+                r.summed.at[p, xb, rows], r.x_in.at[p, rows],
+                r.bx_s.at[p, i], r.bx_r.at[p, i], to_x,
+            )
+        )
+
+    def give_y(p, i, rows):
+        by_copy[p].append(
+            send(
+                r.summed.at[p, yb, rows], r.y_in.at[p, rows],
+                r.by_s.at[p, i], r.by_r.at[p, i], to_y,
+            )
+        )
+
+    def fold(p):
+        back[p].wait_recv()
+        for k in (db, xb, yb, mine):
+            r.summed[p, k] = narrow(wide(r.partial[p, c, k]) + wide(r.core_in[p, k]))
+        dx_copy[p] = send(
+            r.summed.at[p, db, top], r.dx_in.at[p], r.dx_s.at[p], r.dx_r.at[p], to_x
+        )
+        dy_copy[p] = send(
+            r.summed.at[p, db, bottom], r.dy_in.at[p], r.dy_s.at[p], r.dy_r.at[p], to_y
+        )
+        give_x(p, 0, top)
+        give_y(p, 0, bottom)
+
+    def join(p):
+        dx_copy[p].wait_recv()
+        r.summed[p, yb, top] = narrow(wide(r.summed[p, yb, top]) + wide(r.dx_in[p]))
+        give_y(p, 1, top)
+        dy_copy[p].wait_recv()
+        r.summed[p, xb, bottom] = narrow(wide(r.summed[p, xb, bottom]) + wide(r.dy_in[p]))
+        give_x(p, 1, bottom)
+
+    def gather(p):
+        for copy in bx_copy[p] + by_copy[p]:
+            copy.wait_recv()
+        return wide(r.summed[p, mine]) + wide(r.x_in[p]) + wide(r.y_in[p])
+
+    def leave(p):
+        r.home_out[p] = narrow(gather(p))
+        home[p] = send(
+            r.home_out.at[p], r.home_in.at[z], r.b_s.at[p], r.b_r.at[z], to_z[p]
+        )
+
+    with jax.named_scope("spread"):
+        for p in range(1, 4):
+            z_copy[p] = send(block(0, mine), block(0, mine), r.z_s.at[p], r.z_r.at[z], to_z[p])
+        spread(0)
+        cross(0)
+        spread(1)
+        corner(0)
     for load in loads:
         load.wait()
-    with jax.named_scope("own"):
-        await_core(0)
-        back0 = serve(0)
-    with jax.named_scope("near"):
-        for k in range(4):
-            plus[k].wait_recv()
-            if k < 2:
-                far[k] = send(block(1, k), block(1, k), q_s.at[k], q_r.at[k], to_zp)
-            relays[1][k] = relay(1, k)
-            minus[k].wait_recv()
-            if k >= 2:
-                far[k] = send(block(2, k), block(2, k), q_s.at[k], q_r.at[k], to_zm)
-            relays[2][k] = relay(2, k)
-        await_core(1)
-        back1 = serve(1)
-        fold(0, back0)
-        for k in range(4):
-            far[k].wait_recv()
-            relays[3][k] = relay(3, k)
-        await_core(2)
-        back2 = serve(2)
-        fold(1, back1)
-        early_m = send(
-            summed.at[1, half_a], near_in.at[1, half_a], e_s.at[1], e_r.at[1], to_zm
-        )
-    with jax.named_scope("far"):
-        await_core(3)
-        back3 = serve(3)
-        fold(2, back2)
-        early_p = send(
-            summed.at[2, half_b], near_in.at[0, half_b], e_s.at[0], e_r.at[0], to_zp
-        )
-        fold(3, back3)
-        far_p = send(summed.at[3, half_a], far_in.at[0], f_s.at[0], f_r.at[0], to_zp)
-        far_m = send(summed.at[3, half_b], far_in.at[1], f_s.at[1], f_r.at[1], to_zm)
+    with jax.named_scope("serve"):
+        cross(1)
+        spread(2)
+        serve(0)
+        corner(1)
+        cross(2)
+        spread(3)
+        fold(0)
+        serve(1)
+        join(0)
+        corner(2)
+        cross(3)
+        fold(1)
+        serve(2)
+        join(1)
+        corner(3)
+        fold(2)
+        serve(3)
+        leave(1)
+        join(2)
+        fold(3)
+        leave(2)
+        join(3)
+        mixture = gather(0)
+        leave(3)
     with jax.named_scope("back"):
-        far_p.wait_recv()
-        for k in range(2):
-            place = x * PAIR + k
-            summed[2, place] = (wide(summed[2, place]) + wide(far_in[0, k])).astype(jnp.bfloat16)
-        late_p = send(
-            summed.at[2, half_a], near_in.at[0, half_a], l_s.at[0], l_r.at[0], to_zp
-        )
-        far_m.wait_recv()
-        for k in range(2):
-            place = ox * PAIR + k
-            summed[1, place] = (wide(summed[1, place]) + wide(far_in[1, k])).astype(jnp.bfloat16)
-        late_m = send(
-            summed.at[1, half_b], near_in.at[1, half_b], l_s.at[1], l_r.at[1], to_zm
-        )
-
-        def total(place):
-            return wide(summed[0, place]) + wide(near_in[0, place]) + wide(near_in[1, place])
-
-        early_p.wait_recv()
-        early_m.wait_recv()
-        late_m.wait_recv()
-        late_p.wait_recv()
-        for k in range(2):
-            place = ox * PAIR + k
-            summed[0, place] = total(place).astype(jnp.bfloat16)
-        xback = send(summed.at[0, half_b], x_in, rx_s.at[0], rx_r.at[0], to_x)
-        xback.wait_recv()
-        summed[0, blk[1]] = (total(blk[1]) + wide(x_in[oy])).astype(jnp.bfloat16)
-        yback = send(summed.at[0, blk[1]], y_in, ry_s.at[0], ry_r.at[0], to_y)
-        keep = total(mine) + wide(x_in[y])
-        yback.wait_recv()
-        mixture = keep + wide(y_in[...])
-        out[...] = (middle[...] + scale_rows(mixture, gain_moe[...])).astype(out.dtype)
+        for p in range(1, 4):
+            g = groups[p]
+            pltpu.make_async_remote_copy(
+                src_ref=r.home_out.at[p], dst_ref=r.home_in.at[g], send_sem=r.b_s.at[p],
+                recv_sem=r.b_r.at[g], device_id=to_z[p], device_id_type=MESH,
+            ).wait_recv()
+            mixture = mixture + wide(r.home_in[g])
+        r.out[...] = (r.middle[...] + scale_rows(mixture, r.gain_moe[...])).astype(r.out.dtype)
         for copy in started:
             copy.wait_send()
 
@@ -391,38 +419,50 @@
     ff = w_gate.shape[1]
     full = width + tail.shape[1]
     blocks = PAIR * PAIR
+    half = tok // 2
     bf, f32 = jnp.bfloat16, jnp.float32
     dma = pltpu.SemaphoreType.DMA
     here = pl.BlockSpec(memory_space=pltpu.VMEM)
     there = pl.BlockSpec(memory_space=pl.ANY)
-    sems = []
-    for dims in (
-        (3,), (1,), (2,), (2, 4), (4,), (4, 4), (4,), (2,), (2,), (2,), (1,), (1,)
+    scratch = {
+        "wg": pltpu.VMEM((width, ff), bf),
+        "wu": pltpu.VMEM((width, ff), bf),
+        "wd": pltpu.VMEM((ff, width), bf),
+        "pc_in": pltpu.VMEM((PAIR, tok, width), bf),
+        "py_out": pltpu.VMEM((tok, width), bf),
+        "py_in": pltpu.VMEM((tok, width), bf),
+        "got": pltpu.VMEM((RING, PAIR, blocks, tok, full), bf),
+        "middle": pltpu.VMEM((tok, width), f32),
+        "active": pltpu.VMEM((PAIR * blocks * tok, ff), bf),
+        "partial": pltpu.VMEM((RING, PAIR, blocks, tok, width), bf),
+        "core_in": pltpu.VMEM((RING, blocks, tok, width), bf),
+        "summed": pltpu.VMEM((RING, blocks, tok, width), bf),
+        "dx_in": pltpu.VMEM((RING, half, width), bf),
+        "dy_in": pltpu.VMEM((RING, half, width), bf),
+        "x_in": pltpu.VMEM((RING, tok, width), bf),
+        "y_in": pltpu.VMEM((RING, tok, width), bf),
+        "home_out": pltpu.VMEM((RING, tok, width), bf),
+        "home_in": pltpu.VMEM((RING, tok, width), bf),
+        "w_sem": dma((3,)),
+    }
+    for name, dims in (
+        ("pc", (2,)), ("py", (1,)), ("z", (4,)), ("x", (4,)), ("y", (4,)), ("hx", (4,)),
+        ("hy", (4,)), ("c", (4, 4)), ("rc", (4,)), ("dx", (4,)), ("dy", (4,)), ("bx", (4, 2)),
+        ("by", (4, 2)), ("b", (4,)),
     ):
-        sems += [dma(dims), dma(dims)]
+        scratch[name + "_s"] = dma(dims)
+        scratch[name + "_r"] = dma(dims)
+    operands = (
+        "part", "residual", "gain_mix", "gain_pre", "gain_moe", "tail", "wg_hbm", "wu_hbm",
+        "wd_hbm",
+    )
+    names = operands + ("out",) + tuple(scratch)
     return pl.pallas_call(
-        experts_kernel,
+        functools.partial(experts_kernel, names),
         out_shape=jax.ShapeDtypeStruct((tok, width), bf),
         in_specs=[here] * 6 + [there] * 3,
         out_specs=here,
-        scratch_shapes=[
-            pltpu.VMEM((width, ff), bf),
-            pltpu.VMEM((width, ff), bf),
-            pltpu.VMEM((ff, width), bf),
-            pltpu.VMEM((RING, PAIR, blocks, tok, full), bf),
-            pltpu.VMEM((tok, width), f32),
-            pltpu.VMEM((PAIR * blocks * tok, full), bf),
-            pltpu.VMEM((PAIR * blocks * tok, ff), bf),
-            pltpu.VMEM((RING, PAIR, blocks, tok, width), bf),
-            pltpu.VMEM((RING, blocks, tok, width), bf),
-            pltpu.VMEM((RING, blocks, tok, width), bf),
-            pltpu.VMEM((2, PAIR, tok, width), bf),
-            pltpu.VMEM((2, blocks, tok, width), bf),
-            pltpu.VMEM((PAIR, tok, width), bf),
-            pltpu.VMEM((tok, width), bf),
-            dma((3,)),
-        ]
-        + sems,
+        scratch_shapes=list(scratch.values()),
         compiler_params=pltpu.CompilerParams(
             collective_id=1, has_side_effects=True, vmem_limit_bytes=56 << 20
         ),
@@ -519,7 +559,7 @@
     grid_fits = lax.axis_size("sp") == RING * PAIR and lax.axis_size("tp") == PAIR * PAIR
     if grid_fits and local_experts == 1 and capacity >= tok_part:
         return experts_layer(
-            part.reshape(PAIR * PAIR, tok_part, width),
+            part.reshape(PAIR, PAIR, tok_part, width),
             residual,
             gain_mix[None],
             gain_pre[None],

time: 138 us -> 101 us (0.73)
  Pallas kernels: 124 us -> 88.2 us
    pallas_call x1, Pallas kernels: 99.8 us -> 63.7 us  [experts_layer(): pl.pallas_call(functools.partial(experts_kernel, names), out_shape=jax.Sh...]
where the time goes in v1:
time: 101 us
  Pallas kernels  88.2 us (87%)
  local copies, waits for them, and re-layouts  6.26 us (6%)
  other arithmetic  3.31 us (3%)
  matrix products  3.2 us (3%)
    pallas_call x1, Pallas kernels, experts_layer(): pl.pallas_call(functools.partial(experts_kernel, names), out_shape=jax.Sh...  63.7 us
    pallas_call x1, Pallas kernels, gather_sp(): pl.pallas_call(functools.partial(gather_kernel, n), out_shape=jax.ShapeDt...  24.5 us
    unnamed x15, local copies, waits for them, and re-layouts  4.52 us

profile of v1, /device:TPU:0, one launch (start us, length us, event | category | flops | bytes accessed | tf_op | source)
XLA Modules:
  0.0 101.2 jit_solution(728091660468626656)
XLA Ops:
  0.0 0.9 copy.62
  0.9 1.0 copy.42
  1.9 0.7 fusion.22
  2.7 0.1 broadcast_multiply_fusion.1
  2.8 0.1 fusion.24
  3.0 0.1 copy.43
  3.1 0.7 pad_maximum_fusion.own_ref
  3.7 24.5 %gather_kv.1 = bf16[8,128,512]{2,1,0:T(8,128)(2,1)} custom-call(bf16[128,512]{1,0:T(8,128)(2,1)} %pad_maximum_fusion.own_ref), custom_call_target="tpu_custom_call" | custom-call | bytes 16777216 | tf_op jit(solution)/shard_map/gather_kv/pallas_call | solution.py:161
  28.2 1.3 %fusion.27 = (bf16[1024,256]{1,0:T(8,128)(2,1)S(1)}, bf16[1024,256]{1,0:T(8,128)(2,1)S(1)}) fusion(bf16[1024,512]{1,0:T(8,128)(2,1)} %bitcast.64), kind=kLoop, calls=%fused_computation.51 | loop fusion | bytes 2097152 | tf_op jit(solution)/shard_map/slice | solution.py:524
  29.5 0.2 copy.48
  29.7 0.2 copy.59
  29.9 0.2 copy.45
  30.3 0.1 fusion.19
  30.4 0.1 multiply_subtract_fusion
  30.5 0.8 bitcast_reduce_fusion
  31.3 0.6 fusion.1
  31.9 0.9 fusion.15
  32.9 0.6 copy-done
  33.5 1.5 %convolution_convert_fusion = bf16[128,2048]{1,0:T(8,128)(2,1)} fusion(bf16[128,1024]{0,1:T(8,128)(2,1)S(1)} %bitcast.74, bf16[1024,2048]{1,0:T(8,128)(2,1)S(1)} %copy-done), kind=kOutput, calls=%fused_computation.5 | convolution fusion | flops 537133056 | bytes 4980736 | tf_op jit(solution)/shard_map/dot_general | solution.py:555
  35.1 0.1 copy.50
  35.1 0.1 copy.51
  35.2 0.7 pad_maximum_fusion.3.refs_5_
  35.9 63.7 %experts_layer.1 = bf16[32,2048]{1,0:T(8,128)(2,1)} custom-call(bf16[2,2,32,2048]{3,2,1,0:T(8,128)(2,1)} %bitcast.68, bf16[32,2048]{1,0:T(8,128)(2,1)} %refs_1_.1, f32[1,2048]{1,0:T(1,128)} %bitcast.78, f32[1,2048]{1,0:T(1,128)} %bitcast.79, f32[1,2048]{1,0:T(1,128)} %bitcast.80, bf16[32,128]{1,0:T(8,128)(2,1)} %pad_maximum_fusion.3.refs_5_, ...), custom_call_target="tpu_custom_call" | custom-call | tf_op jit(solution)/shard_map/experts_layer/pallas_call | solution.py:460
  99.7 1.6 %copy.64 = bf16[32,2048]{1,0:T(8,128)(2,1)} copy(bf16[32,2048]{1,0:T(8,128)(2,1)} %experts_layer.1) | data formatting | bytes 262144
  (24 shorter events, 0.3 us)
Async XLA Ops:
  0.0 29.9 %copy-start.1 = (bf16[128,8,128]{2,1,0:T(8,128)(2,1)S(1)}, bf16[128,8,128]{2,1,0:T(8,128)(2,1)}, u32[]{:S(2)}) copy-start(bf16[128,8,128]{2,1,0:T(8,128)(2,1)} %param.15) | copy-start | bytes 786436
  0.0 30.2 %copy-start.4 = (f32[128]{0:T(128)S(1)}, f32[128]{0:T(128)}, u32[]{:S(2)}) copy-start(f32[128]{0:T(128)} %param.18) | copy-start | bytes 1540
  31.3 2.2 %copy-start = (bf16[1024,2048]{1,0:T(8,128)(2,1)S(1)}, bf16[1024,2048]{1,0:T(8,128)(2,1)}, u32[]{:S(2)}) copy-start(bf16[1024,2048]{1,0:T(8,128)(2,1)} %param.20) | copy-start | bytes 12582916
  31.9 3.1 %copy-start.2 = (f32[32,4]{0,1:T(4,128)S(1)}, f32[32,4]{0,1:T(4,128)}, u32[]{:S(2)}) copy-start(f32[32,4]{0,1:T(4,128)} %param.25) | copy-start | bytes 1540
  31.9 3.1 %copy-start.3 = (s32[32,4]{0,1:T(4,128)S(1)}, s32[32,4]{0,1:T(4,128)}, u32[]{:S(2)}) copy-start(s32[32,4]{0,1:T(4,128)} %param.24) | copy-start | bytes 1540

commit v2 on v1

--- a/solution.py
+++ b/solution.py
@@ -180,7 +180,7 @@
     return value.astype(jnp.float32)
 
 
-def experts_kernel(names, *refs):
+def layer_kernel(names, *refs):
     r = SimpleNamespace(**dict(zip(names, refs)))
     sp = lax.axis_index("sp")
     tp = lax.axis_index("tp")
@@ -206,87 +206,267 @@
 
     loads = [
         pltpu.make_async_copy(a, b, r.w_sem.at[i])
-        for i, (a, b) in enumerate(((r.wg_hbm, r.wg), (r.wu_hbm, r.wu), (r.wd_hbm, r.wd)))
+        for i, (a, b) in enumerate(
+            ((r.wo_hbm, r.wo), (r.wg_hbm, r.wg), (r.wu_hbm, r.wu), (r.wd_hbm, r.wd))
+        )
     ]
     for load in loads:
         load.start()
     barrier = pltpu.get_barrier_semaphore()
     for peer in peers:
         pl.semaphore_signal(barrier, inc=1, device_id=peer, device_id_type=MESH)
-    pl.semaphore_wait(barrier, len(peers))
-
-    started = []
+
+    started, inner_started = [], []
+    inner = lax.rem(z + 1, RING) > 1
+    outer = lax.rem(z + 1, RING) <= 1
+
+    def remote(src, dst, s, t, to):
+        return pltpu.make_async_remote_copy(
+            src_ref=src, dst_ref=dst, send_sem=s, recv_sem=t, device_id=to, device_id_type=MESH
+        )
 
     def send(src, dst, s, t, to):
-        copy = pltpu.make_async_remote_copy(
-            src_ref=src, dst_ref=dst, send_sem=s, recv_sem=t, device_id=to, device_id_type=MESH
-        )
+        copy = remote(src, dst, s, t, to)
         copy.start()
         started.append(copy)
         return copy
 
+    def passing(ref, s, t, p):
+        return remote(ref, ref, s, t, to_z[1] if p == 2 else to_z[2])
+
     def narrow(value):
         return value.astype(jnp.bfloat16)
 
+    tokens, heads, size = r.queries.shape
+    kv_heads = r.keys.shape[1]
+    kv_cols = kv_heads * size
+    lane = lax.broadcasted_iota(jnp.int32, (tokens, size), 1)
+    place = sp * tokens + lax.broadcasted_iota(jnp.int32, (tokens, size), 0)
+    shift = GRID_W.bit_length() - 1
+    quarter = size // 4
+    index = jnp.where(lane < size // 2, lax.shift_right_logical(place, shift), place & (GRID_W - 1))
+    freq = wide(lane & (quarter - 1))
+    angle = wide(index) * jnp.exp(freq * (-math.log(rope_theta) / quarter))
+    lower = (lane & quarter) == 0
+    cosine = jnp.cos(angle)
+    sine = jnp.where(lower, -jnp.sin(angle), jnp.sin(angle))
+
+    def turned(value, gain):
+        value = scale_rows(wide(value), gain)
+        ahead = pltpu.roll(value, size - quarter, axis=value.ndim - 1)
+        behind = pltpu.roll(value, quarter, axis=value.ndim - 1)
+        if value.ndim == 2:
+            return value * cosine + jnp.where(lower, ahead, behind) * sine
+        low = (lax.broadcasted_iota(jnp.int32, value.shape, 2) & quarter) == 0
+        return value * cosine[:, None] + jnp.where(low, ahead, behind) * sine[:, None]
+
+    with jax.named_scope("keys"):
+        for g in range(kv_heads):
+            cols = pl.ds(g * size, size)
+            r.kv[0, z, x, :, cols] = narrow(turned(r.keys[:, g, :], r.k_gain[...]))
+            r.kv[1, z, x, :, cols] = r.values[:, g, :]
+    pl.semaphore_wait(barrier, len(peers))
+    def kv_at(p, i):
+        return r.kv.at[i, groups[p], x]
+
+    def kv_x(p, i):
+        return remote(kv_at(p, i), kv_at(p, i), r.kx_s.at[p, i], r.kx_r.at[p, i], to_x)
+
+    def kv_z(p, i, to):
+        return remote(
+            kv_at(p, i), kv_at(p, i), r.kz_s.at[p, i], r.kz_r.at[groups[p], i], to
+        )
+
+    def kv_pass(p, i):
+        return passing(kv_at(p, i), r.kf_s.at[p, i], r.kz_r.at[groups[p], i], p)
+
+    def kv_across(p, i):
+        kv_z(p, i, to_z[1]).wait_recv()
+        pl.when(inner)(kv_pass(p, i).start)
+        kv_x(p, i).start()
+
+    for i in range(2):
+        kv_z(0, i, to_z[1]).start()
+        pl.when(inner)(kv_pass(0, i).start)
+        kv_x(0, i).start()
+        started.append(kv_z(0, i, to_z[1]))
+        started.extend(kv_x(p, i) for p in range(4))
+        inner_started.extend(kv_pass(p, i) for p in range(4))
+    with jax.named_scope("queries"):
+        query = turned(r.queries[...], r.q_gain[...]) * size ** (-0.5)
+        group_size = heads // kv_heads
+        owner = lax.broadcasted_iota(jnp.int32, query.shape, 1) // group_size
+        for g in range(kv_heads):
+            r.query[:, pl.ds(g * size, size)] = narrow(
+                jnp.where(owner == g, query, 0.0).reshape(tokens * heads, size)
+            )
+    spot = lax.broadcasted_iota(jnp.int32, (RING * PAIR, LANES), 1)
+    expert = lax.broadcasted_iota(jnp.int32, spot.shape, 0)
+    named = lax.broadcasted_iota(jnp.int32, (RING * PAIR, r.routes.shape[1]), 0)
+    coef = jnp.zeros(named.shape, jnp.float32)
+    for k in range(r.routes.shape[0]):
+        hit = r.routes[k:k + 1, :] == named
+        coef = coef + jnp.where(hit, r.route_weights[k:k + 1, :], 0.0)
+    high = narrow(coef)
+    low = narrow(coef - wide(high))
+
+    def columns(value, offset):
+        pick = narrow(jnp.where(spot == expert + offset, 1.0, 0.0))
+        return lax.dot_general(
+            value, pick, (((0,), (0,)), ((), ())), preferred_element_type=jnp.float32
+        )
+
+    r.got[z, c, mine, :, width:] = narrow(columns(high, 0) + columns(low, LANES // 2))
+    row_step = min(tokens * heads, 256)
+
+    def attend(p):
+        for i in range(2):
+            kv_x(p, i).wait_recv()
+
+        @pl.loop(0, tokens * heads // row_step)
+        def _(i):
+            rows = pl.ds(pl.multiple_of(i * row_step, row_step), row_step)
+            key = r.kv[0, groups[p]].reshape(PAIR * tokens, kv_cols)
+            value = r.kv[1, groups[p]].reshape(PAIR * tokens, kv_cols)
+            scores = lax.dot_general(
+                r.query[rows, :], key, (((1,), (1,)), ((), ())),
+                preferred_element_type=jnp.float32,
+            )
+            top_now = jnp.max(scores, axis=1, keepdims=True)
+            if p:
+                before = r.top[rows, :]
+                top_now = jnp.maximum(before[:, :1], top_now)
+            unnormed = jnp.exp(scores - top_now)
+            total = jnp.sum(unnormed, axis=1, keepdims=True)
+            both = jnp.dot(narrow(unnormed), value, preferred_element_type=jnp.float32)
+            head = lax.rem(lax.broadcasted_iota(jnp.int32, (row_step, size), 0), heads)
+            mixed = both[:, :size]
+            for g in range(1, kv_heads):
+                mixed = jnp.where(
+                    head // group_size == g, both[:, g * size:(g + 1) * size], mixed
+                )
+            if p:
+                rescale = jnp.exp(before - top_now)
+                total = r.total[rows, :] * rescale + total
+                mixed = r.mixed[rows, :] * rescale + mixed
+            if p < 3:
+                r.top[rows, :] = jnp.broadcast_to(top_now, (row_step, size))
+                r.total[rows, :] = jnp.broadcast_to(total, (row_step, size))
+                r.mixed[rows, :] = mixed
+            else:
+                r.mixed[rows, :] = mixed / total
+
+    with jax.named_scope("attend"):
+        for i in range(2):
+            kv_across(1, i)
+            pl.when(inner)(functools.partial(kv_across, 2, i))
+        attend(0)
+        for i in range(2):
+            pl.when(outer)(functools.partial(kv_across, 2, i))
+            pl.when(inner)(functools.partial(kv_across, 3, i))
+        attend(1)
+        for i in range(2):
+            pl.when(outer)(functools.partial(kv_across, 3, i))
+        attend(2)
+        attend(3)
+        for h in range(heads):
+            r.heads[:, pl.ds(h * size, size)] = narrow(
+                r.mixed[pl.ds(h, tokens, stride=heads), :]
+            )
+    loads[0].wait()
+    tok = r.residual.shape[0]
+    pieces = r.pc_s.shape[0]
+    piece = width // pieces
+    pair_copy, y_part = [], []
+    def fold_pair(i):
+        cols = pl.ds(i * piece, piece)
+        pair_copy[i].wait_recv()
+        r.py_out[:, cols] = narrow(wide(r.part[oy, c, :, cols]) + wide(r.pc_in[oy, :, cols]))
+        y_part.append(
+            send(r.py_out.at[:, cols], r.py_in.at[:, cols], r.py_s.at[i], r.py_r.at[i], to_y)
+        )
+
     with jax.named_scope("proj"):
-        first = send(r.part.at[oy, oc], r.pc_in.at[0], r.pc_s.at[0], r.pc_r.at[0], to_c)
-        second = send(r.part.at[y, oc], r.pc_in.at[1], r.pc_s.at[1], r.pc_r.at[1], to_c)
-        first.wait_recv()
-        r.py_out[...] = narrow(wide(r.part[oy, c]) + wide(r.pc_in[0]))
-        third = send(r.py_out, r.py_in, r.py_s.at[0], r.py_r.at[0], to_y)
-        second.wait_recv()
-        projected = wide(r.part[y, c]) + wide(r.pc_in[1])
-        third.wait_recv()
-        projected = projected + wide(r.py_in[...])
+        for i in range(pieces):
+            cols = pl.ds(i * piece, piece)
+            part = jnp.dot(r.heads[...], r.wo[:, cols], preferred_element_type=jnp.float32)
+            r.part[:, :, :, cols] = narrow(part).reshape(PAIR, PAIR, tok, piece)
+            pair_copy.append(
+                send(
+                    r.part.at[:, oc, :, cols], r.pc_in.at[:, :, cols],
+                    r.pc_s.at[i], r.pc_r.at[i], to_c,
+                )
+            )
+            if i:
+                fold_pair(i - 1)
+        fold_pair(pieces - 1)
+        for i in range(pieces):
+            y_part[i].wait_recv()
+        projected = wide(r.part[y, c]) + wide(r.pc_in[y]) + wide(r.py_in[...])
         mid = wide(r.residual[...]) + scale_rows(projected, r.gain_mix[...])
         r.middle[...] = mid
         r.got[z, c, mine, :, 0:width] = narrow(scale_rows(mid, r.gain_pre[...]))
-        r.got[z, c, mine, :, width:] = r.tail[...]
 
     def block(p, k, rows=slice(None)):
         return r.got.at[groups[p], c, k, rows]
 
-    z_copy, x_copy, y_copy = [None] * 4, [None] * 4, [None] * 4
     hx_copy, hy_copy = [None] * 4, [None] * 4
-    relays = [[] for _ in range(4)]
 
     def relay(p, k, slot):
-        relays[p].append(
-            send(block(p, k), block(p, k), r.c_s.at[p, slot], r.c_r.at[p, slot], to_c)
-        )
+        return remote(block(p, k), block(p, k), r.c_s.at[p, slot], r.c_r.at[p, slot], to_c)
+
+    def along_x(p):
+        return remote(block(p, mine), block(p, mine), r.x_s.at[p], r.x_r.at[p], to_x)
+
+    def along_y(p):
+        return remote(block(p, mine), block(p, mine), r.y_s.at[p], r.y_r.at[p], to_y)
+
+    def along_z(p):
+        return remote(
+            block(p, mine), block(p, mine), r.z_s.at[p], r.z_r.at[groups[p]], to_z[1]
+        )
+
+    def block_pass(p):
+        return passing(block(p, mine), r.zf_s.at[p], r.z_r.at[groups[p]], p)
 
     def spread(p):
         if p:
-            pltpu.make_async_remote_copy(
-                src_ref=block(p, mine), dst_ref=block(p, mine), send_sem=r.z_s.at[p],
-                recv_sem=r.z_r.at[groups[p]], device_id=to_z[p], device_id_type=MESH,
-            ).wait_recv()
-        x_copy[p] = send(block(p, mine), block(p, mine), r.x_s.at[p], r.x_r.at[p], to_x)
-        y_copy[p] = send(block(p, mine), block(p, mine), r.y_s.at[p], r.y_r.at[p], to_y)
-        relay(p, mine, 0)
+            along_z(p).wait_recv()
+        else:
+            along_z(p).start()
+        pl.when(inner)(block_pass(p).start)
+        along_x(p).start()
+        along_y(p).start()
+        relay(p, mine, 0).start()
+
+    started.append(along_z(0))
+    for p in range(4):
+        inner_started.append(block_pass(p))
+        started += [along_x(p), along_y(p)]
+        started += [relay(p, k, i) for i, k in enumerate((mine, xb, yb, db))]
 
     def cross(p):
-        x_copy[p].wait_recv()
+        along_x(p).wait_recv()
         hy_copy[p] = send(
             block(p, xb, top), block(p, xb, top), r.hy_s.at[p], r.hy_r.at[p], to_y
         )
-        relay(p, xb, 1)
-        y_copy[p].wait_recv()
+        relay(p, xb, 1).start()
+        along_y(p).wait_recv()
         hx_copy[p] = send(
             block(p, yb, bottom), block(p, yb, bottom), r.hx_s.at[p], r.hx_r.at[p], to_x
         )
-        relay(p, yb, 2)
+        relay(p, yb, 2).start()
 
     def corner(p):
         hx_copy[p].wait_recv()
         hy_copy[p].wait_recv()
-        relay(p, db, 3)
+        relay(p, db, 3).start()
 
     per = r.got.shape[2] * r.got.shape[3]
 
     def serve(p):
-        for copy in relays[p]:
-            copy.wait_recv()
+        for i, k in enumerate((mine, xb, yb, db)):
+            relay(p, k, i).wait_recv()
         g = groups[p]
         spread_w = wide(r.got[g, :, :, :, width:].reshape(2 * per, LANES))
         lane = lax.broadcasted_iota(jnp.int32, spread_w.shape, 1)
@@ -368,21 +548,21 @@
         )
 
     with jax.named_scope("spread"):
-        for p in range(1, 4):
-            z_copy[p] = send(block(0, mine), block(0, mine), r.z_s.at[p], r.z_r.at[z], to_z[p])
         spread(0)
         cross(0)
         spread(1)
+        pl.when(inner)(functools.partial(spread, 2))
         corner(0)
-    for load in loads:
+        pl.when(outer)(functools.partial(spread, 2))
+        pl.when(inner)(functools.partial(spread, 3))
+    for load in loads[1:]:
         load.wait()
     with jax.named_scope("serve"):
+        serve(0)
         cross(1)
-        spread(2)
-        serve(0)
+        pl.when(outer)(functools.partial(spread, 3))
         corner(1)
         cross(2)
-        spread(3)
         fold(0)
         serve(1)
         join(0)
@@ -413,18 +593,37 @@
         for copy in started:
             copy.wait_send()
 
-
-def experts_layer(part, residual, gain_mix, gain_pre, gain_moe, tail, w_gate, w_up, w_down):
+        @pl.when(inner)
+        def _():
+            for copy in inner_started:
+                copy.wait_send()
+
+
+def whole_layer(
+    queries, keys, values, q_gain, k_gain, w_out, residual, gain_mix, gain_pre, routes,
+    route_weights, w_gate, w_up, w_down, gain_moe,
+):
+    tokens, heads, size = queries.shape
+    kv_cols = keys.shape[1] * size
     tok, width = residual.shape
     ff = w_gate.shape[1]
-    full = width + tail.shape[1]
+    full = width + LANES
     blocks = PAIR * PAIR
     half = tok // 2
+    pieces = 2
     bf, f32 = jnp.bfloat16, jnp.float32
     dma = pltpu.SemaphoreType.DMA
     here = pl.BlockSpec(memory_space=pltpu.VMEM)
     there = pl.BlockSpec(memory_space=pl.ANY)
     scratch = {
+        "kv": pltpu.VMEM((2, RING, PAIR, tokens, kv_cols), bf),
+        "query": pltpu.VMEM((tokens * heads, kv_cols), bf),
+        "top": pltpu.VMEM((tokens * heads, size), f32),
+        "total": pltpu.VMEM((tokens * heads, size), f32),
+        "mixed": pltpu.VMEM((tokens * heads, size), f32),
+        "heads": pltpu.VMEM((tokens, heads * size), bf),
+        "wo": pltpu.VMEM((heads * size, width), bf),
+        "part": pltpu.VMEM((PAIR, PAIR, tok, width), bf),
         "wg": pltpu.VMEM((width, ff), bf),
         "wu": pltpu.VMEM((width, ff), bf),
         "wd": pltpu.VMEM((ff, width), bf),
@@ -443,40 +642,34 @@
         "y_in": pltpu.VMEM((RING, tok, width), bf),
         "home_out": pltpu.VMEM((RING, tok, width), bf),
         "home_in": pltpu.VMEM((RING, tok, width), bf),
-        "w_sem": dma((3,)),
+        "w_sem": dma((4,)),
     }
     for name, dims in (
-        ("pc", (2,)), ("py", (1,)), ("z", (4,)), ("x", (4,)), ("y", (4,)), ("hx", (4,)),
+        ("kz", (4, 2)), ("kx", (4, 2)), ("kf", (4, 2)), ("zf", (4,)), ("pc", (pieces,)), ("py", (pieces,)), ("z", (4,)), ("x", (4,)), ("y", (4,)), ("hx", (4,)),
         ("hy", (4,)), ("c", (4, 4)), ("rc", (4,)), ("dx", (4,)), ("dy", (4,)), ("bx", (4, 2)),
         ("by", (4, 2)), ("b", (4,)),
     ):
         scratch[name + "_s"] = dma(dims)
         scratch[name + "_r"] = dma(dims)
     operands = (
-        "part", "residual", "gain_mix", "gain_pre", "gain_moe", "tail", "wg_hbm", "wu_hbm",
-        "wd_hbm",
+        "queries", "keys", "values", "q_gain", "k_gain", "residual", "gain_mix", "gain_pre",
+        "gain_moe", "routes", "route_weights", "wo_hbm", "wg_hbm", "wu_hbm", "wd_hbm",
     )
     names = operands + ("out",) + tuple(scratch)
     return pl.pallas_call(
-        functools.partial(experts_kernel, names),
+        functools.partial(layer_kernel, names),
         out_shape=jax.ShapeDtypeStruct((tok, width), bf),
-        in_specs=[here] * 6 + [there] * 3,
+        in_specs=[here] * 11 + [there] * 4,
         out_specs=here,
         scratch_shapes=list(scratch.values()),
         compiler_params=pltpu.CompilerParams(
             collective_id=1, has_side_effects=True, vmem_limit_bytes=56 << 20
         ),
-        name="experts_layer",
-    )(part, residual, gain_mix, gain_pre, gain_moe, tail, w_gate, w_up, w_down)
-
-
-def weight_tail(routes, route_weights, experts):
-    hits = routes[:, :, None] == jnp.arange(experts, dtype=jnp.int32)[None, None, :]
-    coef = jnp.sum(jnp.where(hits, route_weights[:, :, None], 0.0), axis=1)
-    high = lax.reduce_precision(coef, 8, 7)
-    low = coef - high
-    gap = jnp.zeros((coef.shape[0], LANES // 2 - experts), jnp.float32)
-    return jnp.concatenate([high, gap, low, gap], axis=1).astype(jnp.bfloat16)
+        name="whole_layer",
+    )(
+        queries, keys, values, q_gain, k_gain, residual, gain_mix, gain_pre, gain_moe, routes,
+        route_weights, w_out, w_gate, w_up, w_down,
+    )
 
 
 def on_device(
@@ -496,6 +689,17 @@
     w_down,
     gain_moe,
 ):
+    local_experts = w_gate.shape[0]
+    experts_all = local_experts * lax.axis_size("sp")
+    tok_part, width = residual.shape
+    capacity = max(2, (2 * tok_part * TOP + experts_all - 1) // experts_all)
+    grid_fits = lax.axis_size("sp") == RING * PAIR and lax.axis_size("tp") == PAIR * PAIR
+    if grid_fits and local_experts == 1 and capacity >= tok_part:
+        return whole_layer(
+            queries, keys, values, q_gain[None], k_gain[None], w_out, residual,
+            gain_mix[None], gain_pre[None], routes.T, route_weights.T, w_gate[0], w_up[0],
+            w_down[0], gain_moe[None],
+        )
     tok_rows, head_local, head_size = queries.shape
     kv_local = keys.shape[1]
     group_size = head_local // kv_local
@@ -550,25 +754,7 @@
     running_max, running_sum, weighted = carry_state
     mixed_heads = (weighted / running_sum[..., None]).transpose(2, 0, 1, 3)
     mixed_heads = mixed_heads.reshape(tok_rows, head_local * head_size).astype(jnp.bfloat16)
-    tok_part = residual.shape[0]
-    width = residual.shape[1]
     part = jnp.dot(mixed_heads, w_out, preferred_element_type=jnp.float32).astype(jnp.bfloat16)
-    local_experts = w_gate.shape[0]
-    experts_all = local_experts * lax.axis_size("sp")
-    capacity = max(2, (2 * tok_part * TOP + experts_all - 1) // experts_all)
-    grid_fits = lax.axis_size("sp") == RING * PAIR and lax.axis_size("tp") == PAIR * PAIR
-    if grid_fits and local_experts == 1 and capacity >= tok_part:
-        return experts_layer(
-            part.reshape(PAIR, PAIR, tok_part, width),
-            residual,
-            gain_mix[None],
-            gain_pre[None],
-            gain_moe[None],
-            weight_tail(routes, route_weights, experts_all),
-            w_gate[0],
-            w_up[0],
-            w_down[0],
-        )
     projected = lax.psum_scatter(
         part,
         "tp",

time: 101 us -> 82.6 us (0.82)
  Pallas kernels: 88.2 us -> 80.9 us
  local copies, waits for them, and re-layouts: 6.26 us -> 1.57 us
  other arithmetic: 3.31 us -> 0 us
  matrix products: 3.2 us -> 0 us
    pallas_call x2 -> x1, Pallas kernels: 88.2 us -> 80.9 us  [whole_layer(): pl.pallas_call(functools.partial(layer_kernel, names), out_shape=jax.Shap...]
    dot_general x3 -> x0, matrix products: 3.2 us -> none  [the longest x1 1.53 us: on_device(): jnp.dot(mixed_heads, w_out, preferred_element_type=jnp.float32)]
    unnamed x15 -> x1, local copies, waits for them, and re-layouts: 4.52 us -> 1.57 us
    slice x2 -> x0, local copies, waits for them, and re-layouts: 1.48 us -> none  [the longest x1 1.27 us: on_device(): key_piece = both[:, :kv_cols].reshape(-1, kv_local, head_size)]
    concatenate x2 -> x0, other arithmetic: 1.35 us -> none  [the longest x1 0.68 us: weight_tail(): return jnp.concatenate([high, gap, low, gap], axis=1).astype(jnp.bfloat16)]
where the time goes in v2:
time: 82.6 us; the launch traced here: 82.5 us
  Pallas kernels  80.9 us (98%)
  local copies, waits for them, and re-layouts  1.57 us (2%)
    pallas_call x1, Pallas kernels, whole_layer(): pl.pallas_call(functools.partial(layer_kernel, names), out_shape=jax.Shap...  80.9 us

profile of v2, /device:TPU:0, one launch (start us, length us, event | category | flops | bytes accessed | tf_op | source)
XLA Modules:
  0.0 82.5 jit_solution(4639739893251385018)
XLA Ops:
  0.0 80.9 %whole_layer.1 = bf16[32,2048]{1,0:T(8,128)(2,1)} custom-call(bf16[128,8,128]{2,1,0:T(8,128)(2,1)} %refs_0_.1, bf16[128,2,128]{2,1,0:T(2,128)(2,1)} %refs_1_.1, bf16[128,2,128]{2,1,0:T(2,128)(2,1)} %refs_2_.1, f32[1,128]{1,0:T(1,128)} %bitcast.18, f32[1,128]{1,0:T(1,128)} %bitcast.19, bf16[32,2048]{1,0:T(8,128)(2,1)} %refs_5_.1, f32[1,2048]{1,0:T(1,128)} %bitcast.13, ...), custom_call_target="tpu_custom_call" | custom-call | tf_op jit(solution)/shard_map/whole_layer/pallas_call | solution.py:659
  80.9 1.6 %copy.17 = bf16[32,2048]{1,0:T(8,128)(2,1)} copy(bf16[32,2048]{1,0:T(8,128)(2,1)} %whole_layer.1) | data formatting | bytes 262144

commit v3 on v2

--- a/solution.py
+++ b/solution.py
@@ -207,7 +207,12 @@
     loads = [
         pltpu.make_async_copy(a, b, r.w_sem.at[i])
         for i, (a, b) in enumerate(
-            ((r.wo_hbm, r.wo), (r.wg_hbm, r.wg), (r.wu_hbm, r.wu), (r.wd_hbm, r.wd))
+            (
+                (r.wo_hbm, r.wo),
+                (r.wg_hbm, r.wg.at[0]),
+                (r.wu_hbm, r.wu.at[0]),
+                (r.wd_hbm, r.wd.at[0]),
+            )
         )
     ]
     for load in loads:
@@ -316,14 +321,17 @@
             value, pick, (((0,), (0,)), ((), ())), preferred_element_type=jnp.float32
         )
 
-    r.got[z, c, mine, :, width:] = narrow(columns(high, 0) + columns(low, LANES // 2))
+    r.got[z, mine, :, width:] = narrow(columns(high, 0) + columns(low, LANES // 2))
     row_step = min(tokens * heads, 256)
 
-    def attend(p):
-        for i in range(2):
-            kv_x(p, i).wait_recv()
-
-        @pl.loop(0, tokens * heads // row_step)
+    def attend(p, part):
+        if part != 1:
+            for i in range(2):
+                kv_x(p, i).wait_recv()
+        steps = tokens * heads // row_step
+        span = {0: (0, steps // 2), 1: (steps // 2, steps), 2: (0, steps)}[part]
+
+        @pl.loop(*span)
         def _(i):
             rows = pl.ds(pl.multiple_of(i * row_step, row_step), row_step)
             key = r.kv[0, groups[p]].reshape(PAIR * tokens, kv_cols)
@@ -356,19 +364,30 @@
             else:
                 r.mixed[rows, :] = mixed / total
 
+    shared = []
+
+    def share():
+        for i, ref in enumerate((r.wg, r.wu, r.wd)):
+            loads[i + 1].wait()
+            shared.append(send(ref.at[0], ref.at[1], r.w_s.at[i], r.w_r.at[i], to_c))
+
     with jax.named_scope("attend"):
         for i in range(2):
             kv_across(1, i)
             pl.when(inner)(functools.partial(kv_across, 2, i))
-        attend(0)
-        for i in range(2):
-            pl.when(outer)(functools.partial(kv_across, 2, i))
-            pl.when(inner)(functools.partial(kv_across, 3, i))
-        attend(1)
-        for i in range(2):
-            pl.when(outer)(functools.partial(kv_across, 3, i))
-        attend(2)
-        attend(3)
+        attend(0, 0)
+        pl.when(outer)(functools.partial(kv_across, 2, 0))
+        pl.when(inner)(functools.partial(kv_across, 3, 0))
+        attend(0, 1)
+        pl.when(outer)(functools.partial(kv_across, 2, 1))
+        pl.when(inner)(functools.partial(kv_across, 3, 1))
+        pl.when(outer)(functools.partial(kv_across, 3, 0))
+        share()
+        attend(1, 0)
+        pl.when(outer)(functools.partial(kv_across, 3, 1))
+        attend(1, 1)
+        attend(2, 2)
+        attend(3, 2)
         for h in range(heads):
             r.heads[:, pl.ds(h * size, size)] = narrow(
                 r.mixed[pl.ds(h, tokens, stride=heads), :]
@@ -405,96 +424,124 @@
         projected = wide(r.part[y, c]) + wide(r.pc_in[y]) + wide(r.py_in[...])
         mid = wide(r.residual[...]) + scale_rows(projected, r.gain_mix[...])
         r.middle[...] = mid
-        r.got[z, c, mine, :, 0:width] = narrow(scale_rows(mid, r.gain_pre[...]))
+        r.got[z, mine, :, 0:width] = narrow(scale_rows(mid, r.gain_pre[...]))
 
     def block(p, k, rows=slice(None)):
-        return r.got.at[groups[p], c, k, rows]
-
-    hx_copy, hy_copy = [None] * 4, [None] * 4
-
-    def relay(p, k, slot):
-        return remote(block(p, k), block(p, k), r.c_s.at[p, slot], r.c_r.at[p, slot], to_c)
-
-    def along_x(p):
-        return remote(block(p, mine), block(p, mine), r.x_s.at[p], r.x_r.at[p], to_x)
-
-    def along_y(p):
-        return remote(block(p, mine), block(p, mine), r.y_s.at[p], r.y_r.at[p], to_y)
-
-    def along_z(p):
-        return remote(
-            block(p, mine), block(p, mine), r.z_s.at[p], r.z_r.at[groups[p]], to_z[1]
-        )
-
-    def block_pass(p):
-        return passing(block(p, mine), r.zf_s.at[p], r.z_r.at[groups[p]], p)
-
-    def spread(p):
-        if p:
-            along_z(p).wait_recv()
+        return r.got.at[groups[p], k, rows]
+
+    through = (0, RING - 1)
+
+    ends = (top, bottom)
+
+    def along_x(p, i):
+        ref = block(p, mine, ends[i])
+        return remote(ref, ref, r.x_s.at[p, i], r.x_r.at[p, i], to_x)
+
+    def along_y(p, i):
+        ref = block(p, mine, ends[i])
+        return remote(ref, ref, r.y_s.at[p, i], r.y_r.at[p, i], to_y)
+
+    def along_z(p, i):
+        ref = block(p, mine, ends[i])
+        return remote(ref, ref, r.z_s.at[p, i], r.z_r.at[groups[p], i], to_z[1])
+
+    def block_pass(p, i):
+        return passing(block(p, mine, ends[i]), r.zf_s.at[p, i], r.z_r.at[groups[p], i], p)
+
+    def corner_z(p):
+        return remote(block(p, db), block(p, db), r.d_s.at[p], r.d_r.at[groups[p]], to_z[1])
+
+    def corner_pass(p):
+        return passing(block(p, db), r.df_s.at[p], r.d_r.at[groups[p]], p)
+
+    def half_x(p):
+        ref = block(p, yb, bottom)
+        return remote(ref, ref, r.hx_s.at[p], r.hx_r.at[p], to_x)
+
+    def half_y(p):
+        ref = block(p, xb, top)
+        return remote(ref, ref, r.hy_s.at[p], r.hy_r.at[p], to_y)
+
+    def begin():
+        for i in range(2):
+            along_z(0, i).start()
+            pl.when(inner)(block_pass(0, i).start)
+            along_x(0, i).start()
+            along_y(0, 1 - i).start()
+
+    def spread(p, i):
+        along_z(p, i).wait_recv()
+        pl.when(inner)(block_pass(p, i).start)
+        along_x(p, i).start()
+        along_y(p, i).start()
+
+    started.append(corner_z(0))
+    inner_started += [corner_pass(0), corner_pass(1)]
+    for p in range(4):
+        for i in range(2):
+            inner_started.append(block_pass(p, i))
+            started += [along_x(p, i), along_y(p, i)]
+        if p in through:
+            started += [half_x(p), half_y(p)]
+    started += [along_z(0, 0), along_z(0, 1)]
+
+    def cross_first(p):
+        along_x(p, 0).wait_recv()
+        half_y(p).start()
+        along_y(p, 1).wait_recv()
+        half_x(p).start()
+
+    def cross_rest(p):
+        if p not in through:
+            along_x(p, 0).wait_recv()
+            along_y(p, 1).wait_recv()
+        along_x(p, 1).wait_recv()
+        along_y(p, 0).wait_recv()
+
+    def corner(p):
+        if p in through:
+            half_x(p).wait_recv()
+            half_y(p).wait_recv()
         else:
-            along_z(p).start()
-        pl.when(inner)(block_pass(p).start)
-        along_x(p).start()
-        along_y(p).start()
-        relay(p, mine, 0).start()
-
-    started.append(along_z(0))
-    for p in range(4):
-        inner_started.append(block_pass(p))
-        started += [along_x(p), along_y(p)]
-        started += [relay(p, k, i) for i, k in enumerate((mine, xb, yb, db))]
-
-    def cross(p):
-        along_x(p).wait_recv()
-        hy_copy[p] = send(
-            block(p, xb, top), block(p, xb, top), r.hy_s.at[p], r.hy_r.at[p], to_y
-        )
-        relay(p, xb, 1).start()
-        along_y(p).wait_recv()
-        hx_copy[p] = send(
-            block(p, yb, bottom), block(p, yb, bottom), r.hx_s.at[p], r.hx_r.at[p], to_x
-        )
-        relay(p, yb, 2).start()
-
-    def corner(p):
-        hx_copy[p].wait_recv()
-        hy_copy[p].wait_recv()
-        relay(p, db, 3).start()
-
-    per = r.got.shape[2] * r.got.shape[3]
-
-    def serve(p):
-        for i, k in enumerate((mine, xb, yb, db)):
-            relay(p, k, i).wait_recv()
+            corner_z(p).wait_recv()
+            if p == 1:
+                pl.when(inner)(corner_pass(p).start)
+
+    per = r.got.shape[1] * r.got.shape[2]
+    ff = r.wg.shape[2]
+    coefs = [None] * 4
+
+    def serve_up(p):
         g = groups[p]
-        spread_w = wide(r.got[g, :, :, :, width:].reshape(2 * per, LANES))
-        lane = lax.broadcasted_iota(jnp.int32, spread_w.shape, 1)
-        chosen = lax.rem(lane, LANES // 2) == sp
-        coef = jnp.sum(jnp.where(chosen, spread_w, 0.0), axis=1, keepdims=True)
-        step = min(r.wg.shape[1], 256)
-
-        @pl.loop(0, r.wg.shape[1] // step)
+        spread_w = wide(r.got[g, :, :, width:].reshape(per, LANES))
+        lanes = lax.broadcasted_iota(jnp.int32, spread_w.shape, 1)
+        chosen = lax.rem(lanes, LANES // 2) == sp
+        coefs[p] = jnp.sum(jnp.where(chosen, spread_w, 0.0), axis=1, keepdims=True)
+
+        @pl.loop(0, PAIR)
+        def _(i):
+            rows = r.got[g, :, :, 0:width].reshape(per, width)
+            gate = jnp.dot(rows, r.wg[i], preferred_element_type=jnp.float32)
+            up = jnp.dot(rows, r.wu[i], preferred_element_type=jnp.float32)
+            gate = jnp.minimum(gate, clamp_limit)
+            up = jnp.clip(up, -clamp_limit, clamp_limit)
+            r.active[i] = narrow(gate * jax.nn.sigmoid(swish_alpha * gate) * (up + 1.0))
+
+    def serve_down(p):
+        step = min(width, 1024)
+
+        @pl.loop(0, width // step)
         def _(i):
             cols = pl.ds(pl.multiple_of(i * step, step), step)
-            rows = r.got[g, :, :, :, 0:width].reshape(2 * per, width)
-            gate = jnp.dot(rows, r.wg[:, cols], preferred_element_type=jnp.float32)
-            up = jnp.dot(rows, r.wu[:, cols], preferred_element_type=jnp.float32)
-            gate = jnp.minimum(gate, clamp_limit)
-            up = jnp.clip(up, -clamp_limit, clamp_limit)
-            r.active[:, cols] = narrow(gate * jax.nn.sigmoid(swish_alpha * gate) * (up + 1.0))
-
-        @pl.loop(0, width // 512)
-        def _(i):
-            cols = pl.ds(pl.multiple_of(i * 512, 512), 512)
-            down = jnp.dot(r.active[...], r.wd[:, cols], preferred_element_type=jnp.float32)
-            r.partial[p, :, :, :, cols] = narrow(down * coef).reshape(
-                r.partial.shape[1:4] + (512,)
+            down = jnp.dot(r.active[0], r.wd[0, :, cols], preferred_element_type=jnp.float32)
+            for j in range(1, PAIR):
+                down = down + jnp.dot(
+                    r.active[j], r.wd[j, :, cols], preferred_element_type=jnp.float32
+                )
+            r.summed[p, :, :, cols] = narrow(down * coefs[p]).reshape(
+                r.summed.shape[1:3] + (step,)
             )
 
-        back[p] = send(r.partial.at[p, oc], r.core_in.at[p], r.rc_s.at[p], r.rc_r.at[p], to_c)
-
-    back = [None] * 4
     dx_copy, dy_copy = [None] * 4, [None] * 4
     bx_copy, by_copy = [[] for _ in range(4)], [[] for _ in range(4)]
     home = [None] * 4
@@ -515,18 +562,50 @@
             )
         )
 
+    def corner_home(p):
+        return remote(
+            r.summed.at[p, db], r.corner_in.at[z], r.e_s.at[p], r.e_r.at[z], to_z[p]
+        )
+
     def fold(p):
-        back[p].wait_recv()
-        for k in (db, xb, yb, mine):
-            r.summed[p, k] = narrow(wide(r.partial[p, c, k]) + wide(r.core_in[p, k]))
+        if p == 0:
+            give_x(p, 0, top)
+            give_y(p, 0, bottom)
+        elif p in through:
+            halves(p)
+            give_x(p, 0, top)
+            give_y(p, 0, bottom)
+        else:
+            started.append(corner_home(p))
+            started[-1].start()
+            give_x(p, 0, slice(None))
+            give_y(p, 0, slice(None))
+
+    def halves(p):
         dx_copy[p] = send(
             r.summed.at[p, db, top], r.dx_in.at[p], r.dx_s.at[p], r.dx_r.at[p], to_x
         )
         dy_copy[p] = send(
             r.summed.at[p, db, bottom], r.dy_in.at[p], r.dy_s.at[p], r.dy_r.at[p], to_y
         )
-        give_x(p, 0, top)
-        give_y(p, 0, bottom)
+
+    def feed():
+        def take(p):
+            g = groups[p]
+            remote(
+                r.summed.at[p, db], r.corner_in.at[g], r.e_s.at[p], r.e_r.at[g], to_z[p]
+            ).wait_recv()
+            return wide(r.corner_in[g])
+
+        @pl.when(inner)
+        def _():
+            r.summed[0, db] = narrow(wide(r.summed[0, db]) + take(1) + take(2) + take(3))
+
+        @pl.when(outer)
+        def _():
+            r.summed[0, db] = narrow(wide(r.summed[0, db]) + take(1))
+
+        halves(0)
 
     def join(p):
         dx_copy[p].wait_recv()
@@ -547,40 +626,62 @@
             r.home_out.at[p], r.home_in.at[z], r.b_s.at[p], r.b_r.at[z], to_z[p]
         )
 
+    def corner_out():
+        corner_z(0).start()
+        pl.when(inner)(corner_pass(0).start)
+
+    def on_inner(action, *args):
+        pl.when(inner)(functools.partial(action, *args))
+
+    def on_outer(action, *args):
+        pl.when(outer)(functools.partial(action, *args))
+
     with jax.named_scope("spread"):
-        spread(0)
-        cross(0)
-        spread(1)
-        pl.when(inner)(functools.partial(spread, 2))
+        begin()
+        cross_first(0)
+        spread(1, 0)
+        on_inner(spread, 2, 0)
+        cross_rest(0)
+        spread(1, 1)
+        on_inner(spread, 2, 1)
         corner(0)
-        pl.when(outer)(functools.partial(spread, 2))
-        pl.when(inner)(functools.partial(spread, 3))
-    for load in loads[1:]:
-        load.wait()
+        on_outer(corner_out)
+        on_inner(spread, 3, 0)
+        on_inner(spread, 3, 1)
+        on_inner(corner_out)
+        on_outer(spread, 2, 0)
+        on_outer(spread, 2, 1)
+    for copy in shared:
+        copy.wait_recv()
     with jax.named_scope("serve"):
-        serve(0)
-        cross(1)
-        pl.when(outer)(functools.partial(spread, 3))
+        serve_up(0)
+        serve_down(0)
+        on_outer(spread, 3, 0)
+        on_outer(spread, 3, 1)
+        fold(0)
+        cross_rest(1)
+        cross_rest(2)
         corner(1)
-        cross(2)
-        fold(0)
-        serve(1)
-        join(0)
+        serve_up(1)
+        cross_first(3)
+        serve_down(1)
+        fold(1)
+        cross_rest(3)
         corner(2)
-        cross(3)
-        fold(1)
-        serve(2)
-        join(1)
+        serve_up(2)
+        serve_down(2)
+        fold(2)
         corner(3)
-        fold(2)
-        serve(3)
+        serve_up(3)
         leave(1)
-        join(2)
+        serve_down(3)
         fold(3)
         leave(2)
         join(3)
+        feed()
+        leave(3)
+        join(0)
         mixture = gather(0)
-        leave(3)
     with jax.named_scope("back"):
         for p in range(1, 4):
             g = groups[p]
@@ -610,7 +711,7 @@
     full = width + LANES
     blocks = PAIR * PAIR
     half = tok // 2
-    pieces = 2
+    pieces = 4
     bf, f32 = jnp.bfloat16, jnp.float32
     dma = pltpu.SemaphoreType.DMA
     here = pl.BlockSpec(memory_space=pltpu.VMEM)
@@ -624,29 +725,28 @@
         "heads": pltpu.VMEM((tokens, heads * size), bf),
         "wo": pltpu.VMEM((heads * size, width), bf),
         "part": pltpu.VMEM((PAIR, PAIR, tok, width), bf),
-        "wg": pltpu.VMEM((width, ff), bf),
-        "wu": pltpu.VMEM((width, ff), bf),
-        "wd": pltpu.VMEM((ff, width), bf),
+        "wg": pltpu.VMEM((PAIR, width, ff), bf),
+        "wu": pltpu.VMEM((PAIR, width, ff), bf),
+        "wd": pltpu.VMEM((PAIR, ff, width), bf),
         "pc_in": pltpu.VMEM((PAIR, tok, width), bf),
         "py_out": pltpu.VMEM((tok, width), bf),
         "py_in": pltpu.VMEM((tok, width), bf),
-        "got": pltpu.VMEM((RING, PAIR, blocks, tok, full), bf),
+        "got": pltpu.VMEM((RING, blocks, tok, full), bf),
         "middle": pltpu.VMEM((tok, width), f32),
-        "active": pltpu.VMEM((PAIR * blocks * tok, ff), bf),
-        "partial": pltpu.VMEM((RING, PAIR, blocks, tok, width), bf),
-        "core_in": pltpu.VMEM((RING, blocks, tok, width), bf),
+        "active": pltpu.VMEM((PAIR, blocks * tok, ff), bf),
         "summed": pltpu.VMEM((RING, blocks, tok, width), bf),
         "dx_in": pltpu.VMEM((RING, half, width), bf),
         "dy_in": pltpu.VMEM((RING, half, width), bf),
         "x_in": pltpu.VMEM((RING, tok, width), bf),
+        "corner_in": pltpu.VMEM((RING, tok, width), bf),
         "y_in": pltpu.VMEM((RING, tok, width), bf),
         "home_out": pltpu.VMEM((RING, tok, width), bf),
         "home_in": pltpu.VMEM((RING, tok, width), bf),
         "w_sem": dma((4,)),
     }
     for name, dims in (
-        ("kz", (4, 2)), ("kx", (4, 2)), ("kf", (4, 2)), ("zf", (4,)), ("pc", (pieces,)), ("py", (pieces,)), ("z", (4,)), ("x", (4,)), ("y", (4,)), ("hx", (4,)),
-        ("hy", (4,)), ("c", (4, 4)), ("rc", (4,)), ("dx", (4,)), ("dy", (4,)), ("bx", (4, 2)),
+        ("kz", (4, 2)), ("kx", (4, 2)), ("kf", (4, 2)), ("pc", (pieces,)), ("py", (pieces,)), ("z", (4, 2)), ("x", (4, 2)), ("y", (4, 2)), ("zf", (4, 2)), ("d", (4,)), ("df", (4,)), ("e", (4,)), ("hx", (4,)),
+        ("hy", (4,)), ("w", (3,)), ("dx", (4,)), ("dy", (4,)), ("bx", (4, 2)),
         ("by", (4, 2)), ("b", (4,)),
     ):
         scratch[name + "_s"] = dma(dims)

time: 82.6 us -> 72.1 us (0.87)
  Pallas kernels: 80.9 us -> 70.3 us
    pallas_call x1, Pallas kernels: 80.9 us -> 70.3 us  [whole_layer(): pl.pallas_call(functools.partial(layer_kernel, names), out_shape=jax.Shap...]
where the time goes in v3:
time: 72.1 us; the launch traced here: 71.9 us
  Pallas kernels  70.3 us (98%)
  local copies, waits for them, and re-layouts  1.57 us (2%)
    pallas_call x1, Pallas kernels, whole_layer(): pl.pallas_call(functools.partial(layer_kernel, names), out_shape=jax.Shap...  70.3 us
    unnamed x1, local copies, waits for them, and re-layouts  1.57 us

profile of v3, /device:TPU:0, one launch (start us, length us, event | category | flops | bytes accessed | tf_op | source)
XLA Modules:
  0.0 71.9 jit_solution(3314612004460932331)
XLA Ops:
  0.0 70.3 %whole_layer.1 = bf16[32,2048]{1,0:T(8,128)(2,1)} custom-call(bf16[128,8,128]{2,1,0:T(8,128)(2,1)} %refs_0_.1, bf16[128,2,128]{2,1,0:T(2,128)(2,1)} %refs_1_.1, bf16[128,2,128]{2,1,0:T(2,128)(2,1)} %refs_2_.1, f32[1,128]{1,0:T(1,128)} %bitcast.18, f32[1,128]{1,0:T(1,128)} %bitcast.19, bf16[32,2048]{1,0:T(8,128)(2,1)} %refs_5_.1, f32[1,2048]{1,0:T(1,128)} %bitcast.13, ...), custom_call_target="tpu_custom_call" | custom-call | tf_op jit(solution)/shard_map/whole_layer/pallas_call | solution.py:759
  70.3 1.6 %copy.17 = bf16[32,2048]{1,0:T(8,128)(2,1)} copy(bf16[32,2048]{1,0:T(8,128)(2,1)} %whole_layer.1) | data formatting | bytes 262144

commit v4 on v3

--- a/solution.py
+++ b/solution.py
@@ -208,14 +208,26 @@
         pltpu.make_async_copy(a, b, r.w_sem.at[i])
         for i, (a, b) in enumerate(
             (
-                (r.wo_hbm, r.wo),
                 (r.wg_hbm, r.wg.at[0]),
                 (r.wu_hbm, r.wu.at[0]),
                 (r.wd_hbm, r.wd.at[0]),
+                (r.wo_hbm, r.wo),
             )
         )
     ]
-    for load in loads:
+    small = [
+        pltpu.make_async_copy(a, b, r.q_sem.at[i])
+        for i, (a, b) in enumerate(
+            (
+                (r.queries_hbm, r.queries),
+                (r.residual_hbm, r.residual),
+                (r.mix_hbm, r.gain_mix),
+                (r.pre_hbm, r.gain_pre),
+                (r.moe_hbm, r.gain_moe),
+            )
+        )
+    ]
+    for load in small + loads:
         load.start()
     barrier = pltpu.get_barrier_semaphore()
     for peer in peers:
@@ -265,12 +277,11 @@
         low = (lax.broadcasted_iota(jnp.int32, value.shape, 2) & quarter) == 0
         return value * cosine[:, None] + jnp.where(low, ahead, behind) * sine[:, None]
 
-    with jax.named_scope("keys"):
-        for g in range(kv_heads):
-            cols = pl.ds(g * size, size)
-            r.kv[0, z, x, :, cols] = narrow(turned(r.keys[:, g, :], r.k_gain[...]))
-            r.kv[1, z, x, :, cols] = r.values[:, g, :]
+    spans = [pl.ds(g * size, size) for g in range(kv_heads)]
+    for g, cols in enumerate(spans):
+        r.kv[1, z, x, :, cols] = r.values[:, g, :]
     pl.semaphore_wait(barrier, len(peers))
+
     def kv_at(p, i):
         return r.kv.at[i, groups[p], x]
 
@@ -288,16 +299,28 @@
     def kv_across(p, i):
         kv_z(p, i, to_z[1]).wait_recv()
         pl.when(inner)(kv_pass(p, i).start)
-        kv_x(p, i).start()
-
-    for i in range(2):
+        if p != 2 or i == 0:
+            kv_x(p, i).start()
+        else:
+            pl.when(outer)(kv_x(p, i).start)
+        if p == 2 and i == 0:
+            pl.when(inner)(kv_x(p, 1).start)
+
+    def kv_begin(i):
         kv_z(0, i, to_z[1]).start()
         pl.when(inner)(kv_pass(0, i).start)
         kv_x(0, i).start()
         started.append(kv_z(0, i, to_z[1]))
         started.extend(kv_x(p, i) for p in range(4))
         inner_started.extend(kv_pass(p, i) for p in range(4))
+
+    kv_begin(1)
+    with jax.named_scope("keys"):
+        for g, cols in enumerate(spans):
+            r.kv[0, z, x, :, cols] = narrow(turned(r.keys[:, g, :], r.k_gain[...]))
+    kv_begin(0)
     with jax.named_scope("queries"):
+        small[0].wait()
         query = turned(r.queries[...], r.q_gain[...]) * size ** (-0.5)
         group_size = heads // kv_heads
         owner = lax.broadcasted_iota(jnp.int32, query.shape, 1) // group_size
@@ -305,23 +328,34 @@
             r.query[:, pl.ds(g * size, size)] = narrow(
                 jnp.where(owner == g, query, 0.0).reshape(tokens * heads, size)
             )
-    spot = lax.broadcasted_iota(jnp.int32, (RING * PAIR, LANES), 1)
-    expert = lax.broadcasted_iota(jnp.int32, spot.shape, 0)
-    named = lax.broadcasted_iota(jnp.int32, (RING * PAIR, r.routes.shape[1]), 0)
+    tok = r.residual.shape[0]
+    named = lax.broadcasted_iota(jnp.int32, (RING * PAIR, tok), 0)
     coef = jnp.zeros(named.shape, jnp.float32)
     for k in range(r.routes.shape[0]):
         hit = r.routes[k:k + 1, :] == named
         coef = coef + jnp.where(hit, r.route_weights[k:k + 1, :], 0.0)
-    high = narrow(coef)
-    low = narrow(coef - wide(high))
-
-    def columns(value, offset):
-        pick = narrow(jnp.where(spot == expert + offset, 1.0, 0.0))
-        return lax.dot_general(
-            value, pick, (((0,), (0,)), ((), ())), preferred_element_type=jnp.float32
-        )
-
-    r.got[z, mine, :, width:] = narrow(columns(high, 0) + columns(low, LANES // 2))
+    coef = jnp.concatenate(
+        [coef, jnp.zeros((RING * PAIR, LANES - tok), jnp.float32)], axis=1
+    )
+    for e in range(RING * PAIR):
+        r.rates[z, mine, e] = coef[e:e + 1, :]
+
+    def rates_z(p):
+        ref = r.rates.at[z, mine]
+        return remote(ref, ref, r.az_s.at[p], r.az_r.at[z], to_z[p])
+
+    def rates_from(p):
+        ref = r.rates.at[groups[p], mine]
+        return remote(ref, ref, r.az_s.at[p], r.az_r.at[groups[p]], to_z[p])
+
+    rates_x = remote(
+        r.rates.at[:, mine], r.rates.at[:, mine], r.ax_s.at[0], r.ax_r.at[0], to_x
+    )
+    rates_y = [
+        remote(r.rates.at[:, k], r.rates.at[:, k], r.ay_s.at[i], r.ay_r.at[i], to_y)
+        for i, k in enumerate((mine, xb))
+    ]
+    started += [rates_z(1), rates_z(2), rates_z(3), rates_x] + rates_y
     row_step = min(tokens * heads, 256)
 
     def attend(p, part):
@@ -331,7 +365,7 @@
         steps = tokens * heads // row_step
         span = {0: (0, steps // 2), 1: (steps // 2, steps), 2: (0, steps)}[part]
 
-        @pl.loop(*span)
+        @pl.loop(*span, unroll=True)
         def _(i):
             rows = pl.ds(pl.multiple_of(i * row_step, row_step), row_step)
             key = r.kv[0, groups[p]].reshape(PAIR * tokens, kv_cols)
@@ -366,33 +400,43 @@
 
     shared = []
 
-    def share():
-        for i, ref in enumerate((r.wg, r.wu, r.wd)):
-            loads[i + 1].wait()
-            shared.append(send(ref.at[0], ref.at[1], r.w_s.at[i], r.w_r.at[i], to_c))
+    def share(i):
+        ref = (r.wg, r.wu, r.wd)[i]
+        loads[i].wait()
+        shared.append(send(ref.at[0], ref.at[1], r.w_s.at[i], r.w_r.at[i], to_c))
 
     with jax.named_scope("attend"):
-        for i in range(2):
+        for i in (1, 0):
             kv_across(1, i)
             pl.when(inner)(functools.partial(kv_across, 2, i))
+        share(0)
+        share(1)
         attend(0, 0)
+        share(2)
+        for p in range(1, 4):
+            rates_z(p).start()
+        pl.when(outer)(functools.partial(kv_across, 2, 1))
+        pl.when(inner)(functools.partial(kv_across, 3, 1))
+        attend(0, 1)
         pl.when(outer)(functools.partial(kv_across, 2, 0))
         pl.when(inner)(functools.partial(kv_across, 3, 0))
-        attend(0, 1)
-        pl.when(outer)(functools.partial(kv_across, 2, 1))
-        pl.when(inner)(functools.partial(kv_across, 3, 1))
+        pl.when(outer)(functools.partial(kv_across, 3, 1))
+        attend(1, 0)
         pl.when(outer)(functools.partial(kv_across, 3, 0))
-        share()
-        attend(1, 0)
-        pl.when(outer)(functools.partial(kv_across, 3, 1))
         attend(1, 1)
+        for p in range(1, 4):
+            rates_from(p).wait_recv()
+        rates_x.start()
         attend(2, 2)
         attend(3, 2)
+        rates_x.wait_recv()
+        for copy in rates_y:
+            copy.start()
         for h in range(heads):
             r.heads[:, pl.ds(h * size, size)] = narrow(
                 r.mixed[pl.ds(h, tokens, stride=heads), :]
             )
-    loads[0].wait()
+    loads[3].wait()
     tok = r.residual.shape[0]
     pieces = r.pc_s.shape[0]
     piece = width // pieces
@@ -421,10 +465,12 @@
         fold_pair(pieces - 1)
         for i in range(pieces):
             y_part[i].wait_recv()
+        for load in small[1:]:
+            load.wait()
         projected = wide(r.part[y, c]) + wide(r.pc_in[y]) + wide(r.py_in[...])
         mid = wide(r.residual[...]) + scale_rows(projected, r.gain_mix[...])
         r.middle[...] = mid
-        r.got[z, mine, :, 0:width] = narrow(scale_rows(mid, r.gain_pre[...]))
+        r.got[z, mine] = narrow(scale_rows(mid, r.gain_pre[...]))
 
     def block(p, k, rows=slice(None)):
         return r.got.at[groups[p], k, rows]
@@ -513,14 +559,15 @@
 
     def serve_up(p):
         g = groups[p]
-        spread_w = wide(r.got[g, :, :, width:].reshape(per, LANES))
-        lanes = lax.broadcasted_iota(jnp.int32, spread_w.shape, 1)
-        chosen = lax.rem(lanes, LANES // 2) == sp
-        coefs[p] = jnp.sum(jnp.where(chosen, spread_w, 0.0), axis=1, keepdims=True)
+        shape = (r.got.shape[1], tok, LANES)
+        lanes = lax.broadcasted_iota(jnp.int32, shape, 2)
+        chosen = lanes == lax.broadcasted_iota(jnp.int32, shape, 1)
+        rates = jnp.where(chosen, jnp.broadcast_to(r.rates[g, :, sp], shape), 0.0)
+        coefs[p] = jnp.sum(rates.reshape(per, LANES), axis=1, keepdims=True)
 
         @pl.loop(0, PAIR)
         def _(i):
-            rows = r.got[g, :, :, 0:width].reshape(per, width)
+            rows = r.got[g].reshape(per, width)
             gate = jnp.dot(rows, r.wg[i], preferred_element_type=jnp.float32)
             up = jnp.dot(rows, r.wu[i], preferred_element_type=jnp.float32)
             gate = jnp.minimum(gate, clamp_limit)
@@ -653,6 +700,8 @@
         on_outer(spread, 2, 1)
     for copy in shared:
         copy.wait_recv()
+    for copy in rates_y:
+        copy.wait_recv()
     with jax.named_scope("serve"):
         serve_up(0)
         serve_down(0)
@@ -660,22 +709,22 @@
         on_outer(spread, 3, 1)
         fold(0)
         cross_rest(1)
-        cross_rest(2)
         corner(1)
+        cross_first(3)
         serve_up(1)
-        cross_first(3)
         serve_down(1)
         fold(1)
-        cross_rest(3)
+        cross_rest(2)
         corner(2)
         serve_up(2)
         serve_down(2)
         fold(2)
+        cross_rest(3)
         corner(3)
         serve_up(3)
-        leave(1)
         serve_down(3)
         fold(3)
+        leave(1)
         leave(2)
         join(3)
         feed()
@@ -708,7 +757,6 @@
     kv_cols = keys.shape[1] * size
     tok, width = residual.shape
     ff = w_gate.shape[1]
-    full = width + LANES
     blocks = PAIR * PAIR
     half = tok // 2
     pieces = 4
@@ -731,7 +779,8 @@
         "pc_in": pltpu.VMEM((PAIR, tok, width), bf),
         "py_out": pltpu.VMEM((tok, width), bf),
         "py_in": pltpu.VMEM((tok, width), bf),
-        "got": pltpu.VMEM((RING, blocks, tok, full), bf),
+        "got": pltpu.VMEM((RING, blocks, tok, width), bf),
+        "rates": pltpu.VMEM((RING, blocks, RING * PAIR, 1, LANES), f32),
         "middle": pltpu.VMEM((tok, width), f32),
         "active": pltpu.VMEM((PAIR, blocks * tok, ff), bf),
         "summed": pltpu.VMEM((RING, blocks, tok, width), bf),
@@ -742,24 +791,30 @@
         "y_in": pltpu.VMEM((RING, tok, width), bf),
         "home_out": pltpu.VMEM((RING, tok, width), bf),
         "home_in": pltpu.VMEM((RING, tok, width), bf),
+        "queries": pltpu.VMEM(queries.shape, bf),
+        "residual": pltpu.VMEM(residual.shape, bf),
+        "gain_mix": pltpu.VMEM(gain_mix.shape, f32),
+        "gain_pre": pltpu.VMEM(gain_pre.shape, f32),
+        "gain_moe": pltpu.VMEM(gain_moe.shape, f32),
+        "q_sem": dma((5,)),
         "w_sem": dma((4,)),
     }
     for name, dims in (
         ("kz", (4, 2)), ("kx", (4, 2)), ("kf", (4, 2)), ("pc", (pieces,)), ("py", (pieces,)), ("z", (4, 2)), ("x", (4, 2)), ("y", (4, 2)), ("zf", (4, 2)), ("d", (4,)), ("df", (4,)), ("e", (4,)), ("hx", (4,)),
-        ("hy", (4,)), ("w", (3,)), ("dx", (4,)), ("dy", (4,)), ("bx", (4, 2)),
+        ("hy", (4,)), ("w", (3,)), ("az", (4,)), ("ax", (1,)), ("ay", (2,)), ("dx", (4,)), ("dy", (4,)), ("bx", (4, 2)),
         ("by", (4, 2)), ("b", (4,)),
     ):
         scratch[name + "_s"] = dma(dims)
         scratch[name + "_r"] = dma(dims)
     operands = (
-        "queries", "keys", "values", "q_gain", "k_gain", "residual", "gain_mix", "gain_pre",
-        "gain_moe", "routes", "route_weights", "wo_hbm", "wg_hbm", "wu_hbm", "wd_hbm",
+        "keys", "values", "q_gain", "k_gain", "routes", "route_weights", "queries_hbm",
+        "residual_hbm", "mix_hbm", "pre_hbm", "moe_hbm", "wo_hbm", "wg_hbm", "wu_hbm", "wd_hbm",
     )
     names = operands + ("out",) + tuple(scratch)
     return pl.pallas_call(
         functools.partial(layer_kernel, names),
         out_shape=jax.ShapeDtypeStruct((tok, width), bf),
-        in_specs=[here] * 11 + [there] * 4,
+        in_specs=[here] * 6 + [there] * 9,
         out_specs=here,
         scratch_shapes=list(scratch.values()),
         compiler_params=pltpu.CompilerParams(
@@ -767,8 +822,8 @@
         ),
         name="whole_layer",
     )(
-        queries, keys, values, q_gain, k_gain, residual, gain_mix, gain_pre, gain_moe, routes,
-        route_weights, w_out, w_gate, w_up, w_down,
+        keys, values, q_gain, k_gain, routes, route_weights, queries, residual, gain_mix,
+        gain_pre, gain_moe, w_out, w_gate, w_up, w_down,
     )
 
 

time: 72.1 us -> 69.3 us (0.961)
  Pallas kernels: 70.3 us -> 67.6 us
    pallas_call x1, Pallas kernels: 70.3 us -> 67.6 us  [whole_layer(): pl.pallas_call(functools.partial(layer_kernel, names), out_shape=jax.Shap...]
where the time goes in v4:
time: 69.3 us; the launch traced here: 69.2 us
  Pallas kernels  67.6 us (98%)
  local copies, waits for them, and re-layouts  1.57 us (2%)
    pallas_call x1, Pallas kernels, whole_layer(): pl.pallas_call(functools.partial(layer_kernel, names), out_shape=jax.Shap...  67.6 us
    unnamed x1, local copies, waits for them, and re-layouts  1.57 us

profile of v4, /device:TPU:0, one launch (start us, length us, event | category | flops | bytes accessed | tf_op | source)
XLA Modules:
  0.0 69.2 jit_solution(9010553229913717036)
XLA Ops:
  0.0 67.6 %whole_layer.1 = bf16[32,2048]{1,0:T(8,128)(2,1)} custom-call(bf16[128,2,128]{2,1,0:T(2,128)(2,1)} %refs_0_.1, bf16[128,2,128]{2,1,0:T(2,128)(2,1)} %refs_1_.1, f32[1,128]{1,0:T(1,128)} %bitcast.18, f32[1,128]{1,0:T(1,128)} %bitcast.19, s32[4,32]{1,0:T(4,128)} %bitcast.16, f32[4,32]{1,0:T(4,128)} %bitcast.17, bf16[128,8,128]{2,1,0:T(8,128)(2,1)} %refs_6_.1, ...), custom_call_target="tpu_custom_call" | custom-call | tf_op jit(solution)/shard_map/whole_layer/pallas_call | solution.py:814
  67.6 1.6 %copy.17 = bf16[32,2048]{1,0:T(8,128)(2,1)} copy(bf16[32,2048]{1,0:T(8,128)(2,1)} %whole_layer.1) | data formatting | bytes 262144

commit v5 on v4

--- a/solution.py
+++ b/solution.py
@@ -730,15 +730,18 @@
         feed()
         leave(3)
         join(0)
-        mixture = gather(0)
+
+        def arrived(p):
+            g = groups[p]
+            remote(
+                r.home_out.at[p], r.home_in.at[g], r.b_s.at[p], r.b_r.at[g], to_z[p]
+            ).wait_recv()
+            return wide(r.home_in[g])
+
+        near = arrived(1) + arrived(2)
+        mixture = near + gather(0)
     with jax.named_scope("back"):
-        for p in range(1, 4):
-            g = groups[p]
-            pltpu.make_async_remote_copy(
-                src_ref=r.home_out.at[p], dst_ref=r.home_in.at[g], send_sem=r.b_s.at[p],
-                recv_sem=r.b_r.at[g], device_id=to_z[p], device_id_type=MESH,
-            ).wait_recv()
-            mixture = mixture + wide(r.home_in[g])
+        mixture = mixture + arrived(3)
         r.out[...] = (r.middle[...] + scale_rows(mixture, r.gain_moe[...])).astype(r.out.dtype)
         for copy in started:
             copy.wait_send()

time: 69.3 us -> 69.4 us (level)
  no operation moved by 1% of the time
where the time goes in v5:
time: 69.4 us; the launch traced here: 69.2 us
  Pallas kernels  67.7 us (98%)
  local copies, waits for them, and re-layouts  1.57 us (2%)
    pallas_call x1, Pallas kernels, whole_layer(): pl.pallas_call(functools.partial(layer_kernel, names), out_shape=jax.Shap...  67.7 us
    unnamed x1, local copies, waits for them, and re-layouts  1.57 us

profile of v5, /device:TPU:0, one launch (start us, length us, event | category | flops | bytes accessed | tf_op | source)
XLA Modules:
  0.0 69.2 jit_solution(10457413594012393008)
XLA Ops:
  0.0 67.7 %whole_layer.1 = bf16[32,2048]{1,0:T(8,128)(2,1)} custom-call(bf16[128,2,128]{2,1,0:T(2,128)(2,1)} %refs_0_.1, bf16[128,2,128]{2,1,0:T(2,128)(2,1)} %refs_1_.1, f32[1,128]{1,0:T(1,128)} %bitcast.18, f32[1,128]{1,0:T(1,128)} %bitcast.19, s32[4,32]{1,0:T(4,128)} %bitcast.16, f32[4,32]{1,0:T(4,128)} %bitcast.17, bf16[128,8,128]{2,1,0:T(8,128)(2,1)} %refs_6_.1, ...), custom_call_target="tpu_custom_call" | custom-call | tf_op jit(solution)/shard_map/whole_layer/pallas_call | solution.py:817
  67.7 1.6 %copy.17 = bf16[32,2048]{1,0:T(8,128)(2,1)} copy(bf16[32,2048]{1,0:T(8,128)(2,1)} %whole_layer.1) | data formatting | bytes 262144
